TPU v7x, 256 devices: a whole 4x4x8 slice. The times are simulated.
256 devices in a mesh: fs: 32 (over z, y), tp: 8 (over x, core).
Axes of the slice: x: 4, y: 4, z: 8, core: 2. Of those that a mesh axis runs over, the one named last changes fastest.
Arguments:
- tokens: bfloat16 [12288, 2048], P(('fs', 'tp')), may hold values from -6 to 6
- ffn1_gain: float32 [2048], replicated, may hold values from 0.1 to 1.9
- ffn1_gate: bfloat16 [2048, 5632], P('fs', 'tp'), may hold values from -0.125 to 0.125
- ffn1_up: bfloat16 [2048, 5632], P('fs', 'tp'), may hold values from -0.125 to 0.125
- ffn1_down: bfloat16 [5632, 2048], P('tp', 'fs'), may hold values from -0.078125 to 0.078125
- mix_gain: float32 [2048], replicated, may hold values from 0.1 to 1.9
- lru_in_weight: bfloat16 [2048, 1536], P('fs', 'tp'), may hold values from -0.125 to 0.125
- lru_gate_weight: bfloat16 [2048, 1536], P('fs', 'tp'), may hold values from -0.125 to 0.125
- conv_weight: bfloat16 [4, 1536], P(None, 'tp'), may hold values from -3 to 3
- gate_a_weight: bfloat16 [24, 64, 64], P('tp'), may hold values from -0.75 to 0.75
- gate_x_weight: bfloat16 [24, 64, 64], P('tp'), may hold values from -0.75 to 0.75
- decay_param: float32 [1536], P('tp'), may hold values from 3.7 to 9
- mix_out_weight: bfloat16 [1536, 2048], P('tp', 'fs'), may hold values from -0.15625 to 0.15625
- ffn2_gain: float32 [2048], replicated, may hold values from 0.1 to 1.9
- ffn2_gate: bfloat16 [2048, 5632], P('fs', 'tp'), may hold values from -0.125 to 0.125
- ffn2_up: bfloat16 [2048, 5632], P('fs', 'tp'), may hold values from -0.125 to 0.125
- ffn2_down: bfloat16 [5632, 2048], P('tp', 'fs'), may hold values from -0.078125 to 0.078125
Outputs:
- layer_out: bfloat16 [12288, 2048], P(('fs', 'tp'))
All inputs are finite; a program needn't handle non-finite values.
Results may differ from a plain program's by a relative error of at most 0.017.
Values may be sent and summed in bfloat16 or wider, within the bound.
No kernel may reach another device: no remote copies, remote signals or barrier semaphores. Data moves between devices by JAX's collectives and lax.ppermute only.
A program may use at most 64 MiB of HBM per device.

v0:
```python
import jax
import jax.numpy as jnp
from jax import lax
from jax.experimental import pallas as pl
from jax.experimental.pallas import tpu as pltpu
from jax.sharding import Mesh
from jax.sharding import PartitionSpec as P

FS = ("z", "y")
TP = ("x", "c")
FS_TP = ("z", "y", "x", "c")

EPS = 1e-06
LANES = 128
SHARD = 64
HALF = 64
WIDE = 256
FFN_LOOPED = (False, True)
PARAMS = pltpu.CompilerParams(vmem_limit_bytes=24 << 20)


def moved(value, axis, by):
    count = lax.axis_size(axis)
    return lax.ppermute(value, axis, [(i, (i - by) % count) for i in range(count)])


def in_vmem(*values):
    return tuple(pltpu.with_memory_space_constraint(v, pltpu.VMEM) for v in values)


def vmem_specs(count):
    return [pl.BlockSpec(memory_space=pltpu.VMEM)] * count


def vmem_call(kernel, out_shape, scratch=()):
    def call(*args):
        return pl.pallas_call(
            kernel,
            in_specs=vmem_specs(len(args)),
            out_specs=jax.tree.map(lambda _: vmem_specs(1)[0], out_shape),
            out_shape=out_shape,
            scratch_shapes=list(scratch),
            compiler_params=PARAMS,
        )(*in_vmem(*args))

    return call


def norm_of(wide, gain):
    scale = lax.rsqrt(jnp.mean(wide * wide, axis=-1, keepdims=True) + EPS)
    return (wide * scale * gain).astype(jnp.bfloat16)


def turned_by_y(values, amount):
    groups = range(0, values.shape[1], WIDE)
    return jnp.concatenate([pltpu.roll(values[:, g : g + WIDE], amount, 1) for g in groups], axis=1)


def turned_to(values, axes):
    z, y = lax.axis_index("z"), lax.axis_index("y")
    if "z" in axes:
        values = pltpu.roll(values, lax.rem(8 - z, 8) * WIDE, 1)
    if "y" in axes:
        values = turned_by_y(values, lax.rem(4 - y, 4) * SHARD)
    return values


def turned_back(values, axes):
    z, y = lax.axis_index("z"), lax.axis_index("y")
    if "y" in axes:
        values = turned_by_y(values, y * SHARD)
    if "z" in axes:
        values = pltpu.roll(values, z * WIDE, 1)
    return values


def turned_norm_of(wide, gain, axes):
    normed = norm_of(wide, gain)
    if axes:
        normed = turned_to(normed.astype(jnp.float32), axes).astype(jnp.bfloat16)
    return normed


def norm_kernel(rows_ref, gain_ref, out_ref):
    out_ref[...] = turned_norm_of(rows_ref[...].astype(jnp.float32), gain_ref[...], "zy")


def turned_norm(values, gain):
    out = pltpu.VMEM(values.shape, jnp.bfloat16)
    return vmem_call(norm_kernel, out)(values, gain[None])


def gather_rows(own):
    mine = lax.all_gather(own, "x", axis=0, tiled=True)
    return mine, moved(mine, "c", 1)


def pair_sum_kernel(mine_ref, other_ref, out_ref):
    rows = out_ref.shape[1]
    for n in range(out_ref.shape[0]):
        own = slice(n * rows, (n + 1) * rows)
        out_ref[n] = (
            mine_ref[own].astype(jnp.float32) + other_ref[own].astype(jnp.float32)
        ).astype(jnp.bfloat16)


def sent_sums(terms):
    mine, other = terms
    count = lax.axis_size("x")
    out = pltpu.VMEM((count, mine.shape[0] // count, mine.shape[1]), jnp.bfloat16)
    other = moved(other, "c", 1)
    sums = vmem_call(pair_sum_kernel, out)(mine, other)
    return lax.all_to_all(sums, "x", split_axis=0, concat_axis=0, tiled=True)


def combine_kernel(half, turned, turn, base_ref, sums_ref, *refs):
    total = sums_ref[0].astype(jnp.float32)
    for n in range(1, sums_ref.shape[0]):
        total = total + sums_ref[n].astype(jnp.float32)
    total = turned_back(total, turned)
    if half:
        total = 0.5 * total
    result = (base_ref[...].astype(jnp.float32) + total).astype(jnp.bfloat16)
    if len(refs) == 1:
        refs[0][...] = result
    else:
        gain_ref, out_ref, norm_ref = refs
        out_ref[...] = result
        norm_ref[...] = turned_norm_of(result.astype(jnp.float32), gain_ref[...], turn)


def combined(base, sums, half, turned="", gain=None, turn=""):
    shape = pltpu.VMEM(base.shape, jnp.bfloat16)
    extra = () if gain is None else (gain[None],)
    outs = [shape] * 2 if extra else [jax.ShapeDtypeStruct(base.shape, jnp.bfloat16)]
    kernel = lambda *refs: combine_kernel(half, turned, turn, *refs)
    return vmem_call(kernel, outs)(base, sums, *extra)


def pack_kernel(plan, out_copies, counts, *refs):
    in_refs, out_refs = refs[: -len(counts)], refs[-len(counts) :]
    places = [
        (ref, k, copies)
        for ref, count, copies in zip(out_refs, counts, out_copies)
        for k in range(count)
    ]
    for (out_ref, n, copies), parts in zip(places, plan):
        pieces = [in_refs[which][:, at : at + size] for which, at, size in parts]
        if len(pieces) == 2:
            low, high = (p.astype(jnp.float32) for p in pieces)
            tile = jnp.concatenate([low, high], axis=1).astype(jnp.bfloat16)
        else:
            tile = pieces[0]
        size = tile.shape[1]
        for at in [()] if copies == 1 else [(k,) for k in range(copies)]:
            if size < LANES:
                out_ref[(*at, n)] = jnp.zeros((SHARD, LANES), jnp.bfloat16)
            out_ref[(*at, n, slice(None), slice(0, size))] = tile


def packed_tiles(plan, arrays, counts, out_copies):
    shapes = [
        jax.ShapeDtypeStruct((*((k,) if k > 1 else ()), n, SHARD, LANES), jnp.bfloat16)
        for n, k in zip(counts, out_copies)
    ]
    return pl.pallas_call(
        lambda *refs: pack_kernel(plan, out_copies, counts, *refs),
        out_shape=shapes,
        compiler_params=PARAMS,
        name="pack",
    )(*[in_hbm(a) for a in arrays])


def gather_tiles(plan, arrays):
    (packed,) = packed_tiles(plan, arrays, (len(plan),), (1,))
    full = lax.all_gather(packed.reshape(-1, LANES), FS, axis=0, tiled=True)
    return full.reshape(-1, len(plan), SHARD, LANES)


def full_tiles(which, count):
    return [((which, k * LANES, LANES),) for k in range(count)]


def after(value, *others):
    return lax.optimization_barrier((value, *others))[0]


def in_hbm(value):
    return pltpu.with_memory_space_constraint(value, pltpu.HBM)


def both_ways(up, down, axis):
    return lax.optimization_barrier((moved(up, axis, 1), moved(down, axis, -1)))


def spread_z_last(block, *others):
    up = down = after(block, *others)
    ups, downs = [block], []
    for _ in range(1, 4):
        up, down = both_ways(up, down, "z")
        ups.append(up)
        downs.insert(0, down)
    return [*ups, moved(up, "z", 1), *downs]


def join_kernel(*refs):
    *part_refs, out_ref = refs
    for n, ref in enumerate(part_refs):
        out_ref[n] = ref[...]


def spread_over_z(own):
    up = down = own
    ups, downs = [own], []
    for _ in range(1, 4):
        up, down = both_ways(up, down, "z")
        ups.append(up)
        downs.insert(0, down)
    parts = [*ups, moved(up, "z", 1), *downs]
    out = pltpu.VMEM((8, *own.shape), jnp.bfloat16)
    return vmem_call(join_kernel, out)(*parts), up, down


def spread_over_y(block):
    up, down = both_ways(block, block, "y")
    cut = (block.shape[1] + 1) // 2
    across = [moved(up[:, :cut], "y", 1), moved(down[:, cut:], "y", -1)]
    return [block, up, *across, down]


def nt_dot(a, b):
    return lax.dot_general(a, b, (((1,), (1,)), ((), ())), preferred_element_type=jnp.float32)


def steps(count, step, looped):
    if looped:
        lax.fori_loop(0, count, lambda n, carry: (step(n), carry)[1], 0)
    else:
        for n in range(count):
            step(n)


def lanes(n, size):
    return pl.ds(n * size if isinstance(n, int) else pl.multiple_of(n * size, size), size)


def ffn_steps(looped, tile, down, mine_ref, other_ref, out_mine_ref, out_other_ref, hidden_ref, rows_ref):
    half = mine_ref.shape[0]
    rows_ref[:half] = mine_ref[...]
    rows_ref[half:] = other_ref[...]

    def hidden_step(n):
        both = jnp.concatenate([tile(n), tile(5 + n)], axis=1)
        pair = jnp.dot(rows_ref[...], both, preferred_element_type=jnp.float32)
        hidden = pair[:, :LANES] * jax.nn.sigmoid(pair[:, :LANES]) * pair[:, LANES:]
        hidden_ref[:, lanes(n, LANES)] = hidden.astype(jnp.bfloat16)

    steps(5, hidden_step, looped[0])
    pair = jnp.dot(rows_ref[...], tile(10), preferred_element_type=jnp.float32)
    hidden = pair * jax.nn.sigmoid(pair) * pltpu.roll(pair, HALF, 1)
    lane = lax.broadcasted_iota(jnp.int32, hidden.shape, 1)
    hidden_ref[:, 5 * LANES :] = jnp.where(lane < HALF, hidden, 0.0).astype(jnp.bfloat16)

    def down_step(n):
        both = jnp.concatenate([down(k, n) for k in range(6)], axis=1)
        terms = nt_dot(hidden_ref[...], both).astype(jnp.bfloat16)
        out_mine_ref[:, lanes(n, WIDE)] = terms[:half]
        out_other_ref[:, lanes(n, WIDE)] = terms[half:]

    steps(8, down_step, looped[1])


def first_ffn_kernel(mine_ref, other_ref, *refs):
    a_refs, b_refs = refs[:8], refs[8:13]
    y = lax.axis_index("y")
    cut = b_refs[2].shape[1]

    def block_a(k, n):
        return jnp.concatenate([a_refs[n][lax.rem(y + q, 4), k] for q in range(4)], axis=0)

    def block_b(k, n):
        across = b_refs[2][n, k] if k < cut else b_refs[3][n, k - cut]
        return jnp.concatenate([b_refs[0][n, k], b_refs[1][n, k], across, b_refs[4][n, k]], axis=0)

    def tile(k):
        block, which = (block_a, 6 + k) if k < 2 else (block_b, k - 2)
        return jnp.concatenate([block(which, n) for n in range(8)], axis=0)

    ffn_steps((False, False), tile, block_a, mine_ref, other_ref, *refs[13:])


def ffn_kernel(mine_ref, other_ref, packed_ref, *refs):
    def down(k, n):
        return packed_ref[pl.ds(n * 4, 4), k].reshape(-1, LANES)

    ffn_steps(FFN_LOOPED, lambda k: packed_ref[:, 6 + k].reshape(-1, LANES), down, mine_ref, other_ref, *refs)


def ffn_terms(rows, kernel, weights):
    half, width = rows[0].shape
    scratch = [
        pltpu.VMEM((2 * half, 6 * LANES), jnp.bfloat16),
        pltpu.VMEM((2 * half, width), jnp.bfloat16),
    ]
    outs = [pltpu.VMEM((half, width), jnp.bfloat16)] * 2
    return vmem_call(kernel, outs, scratch)(*rows, *weights)


def shifted(values, by, fill):
    row = lax.broadcasted_iota(jnp.int32, values.shape, 0)
    return jnp.where(row >= by, pltpu.roll(values, by, 0), fill)


def minus_expm1(x):
    series = 1.0 + x / 8.0
    for k in range(7, 1, -1):
        series = 1.0 + (x / k) * series
    return jnp.where(x > -0.5, -x * series, 1.0 - jnp.exp(x))


def scanned(keep, drive):
    by = 1
    while by < keep.shape[0]:
        drive = keep * shifted(drive, by, 0.0) + drive
        keep = keep * shifted(keep, by, 1.0)
        by *= 2
    return drive


def mixer_kernel(
    mine_ref, other_ref, packed_ref, taps_ref, a_ref, b_ref, rate_ref, out_mine_ref, out_other_ref, order_ref
):
    half = mine_ref.shape[0]
    chips = lax.axis_size("x")
    block = half // chips
    core = lax.axis_index("c")


    def tile(k, n):
        return packed_ref[pl.ds(n * 4, 4), k].reshape(-1, LANES)

    weights = [jnp.concatenate([tile(k, n) for n in range(8)], axis=0) for k in range(3)]
    weights = jnp.concatenate(weights, axis=1)
    places = []
    for n, ref in enumerate((mine_ref, other_ref)):
        part = jnp.dot(ref[...], weights, preferred_element_type=jnp.float32)
        which = core if n == 0 else 1 - core
        for chip in range(chips):
            place = pl.multiple_of((chip * 2 + which) * block, block)
            places.append(place)
            order_ref[pl.ds(place, block), :] = part[chip * block : (chip + 1) * block]
    z = order_ref[:, : 2 * LANES]
    ends = order_ref[:, 2 * LANES :]
    lane = lax.broadcasted_iota(jnp.int32, ends.shape, 1)
    groups = (
        (z[:, :LANES], z[:, LANES:]),
        (jnp.where(lane < HALF, ends, 0.0), pltpu.roll(ends, HALF, 1)),
    )
    mixed = []
    for g, (lru_x, lru_gate) in enumerate(groups):
        lru_x = lru_x.astype(jnp.bfloat16).astype(jnp.float32)
        lru_gate = lru_gate.astype(jnp.bfloat16).astype(jnp.float32)
        own = slice(g * LANES, (g + 1) * LANES)
        taps = taps_ref[:, own]
        conv = taps[0:1] * lru_x
        for k in range(1, 4):
            conv = conv + taps[k : k + 1] * shifted(lru_x, k, 0.0)
        low = conv.astype(jnp.bfloat16)
        recall = jax.nn.sigmoid(jnp.dot(low, a_ref[g], preferred_element_type=jnp.float32))
        admit = jax.nn.sigmoid(jnp.dot(low, b_ref[g], preferred_element_type=jnp.float32))
        log_keep = recall * rate_ref[:, own]
        drive = jnp.sqrt(minus_expm1(2.0 * log_keep)) * admit * low.astype(jnp.float32)
        state = scanned(jnp.exp(log_keep), drive)
        mixed.append(state * jax.nn.gelu(lru_gate))
    for g in range(2):
        order_ref[:, g * LANES : (g + 1) * LANES] = mixed[g]
    mixed = jnp.concatenate([order_ref[pl.ds(p, block), : 2 * LANES] for p in places], axis=0)
    mixed = mixed.astype(jnp.bfloat16)
    full = mixed[:, :LANES]
    short = mixed[:, LANES : LANES + HALF]

    def out_step(n):
        terms = nt_dot(full, tile(3, n)) + nt_dot(short, tile(4, n)[:, :HALF])
        terms = terms.astype(jnp.bfloat16)
        out_mine_ref[:, lanes(n, WIDE)] = terms[:half]
        out_other_ref[:, lanes(n, WIDE)] = terms[half:]

    steps(8, out_step, True)


def paired_blocks(blocks):
    zero = jnp.zeros_like(blocks[0])
    top = jnp.concatenate(
        [jnp.concatenate([blocks[0], zero], 1), jnp.concatenate([zero, blocks[1]], 1)], 0
    )
    end = jnp.concatenate(
        [jnp.concatenate([blocks[2], zero], 1), jnp.concatenate([zero, zero], 1)], 0
    )
    return jnp.stack([top, end])


def mixer_terms(rows, packed, conv_weight, gate_a_weight, gate_x_weight, decay_param):
    half, width = rows[0].shape
    pad = ((0, 0), (0, HALF))
    taps = jnp.pad(conv_weight.astype(jnp.float32), pad)
    rate = jnp.pad(-8.0 * jax.nn.softplus(-decay_param)[None], pad)
    outs = [pltpu.VMEM((half, width), jnp.bfloat16)] * 2
    scratch = [pltpu.VMEM((2 * half, 3 * LANES), jnp.float32)]
    return vmem_call(mixer_kernel, outs, scratch)(
        *rows, packed, taps, paired_blocks(gate_a_weight), paired_blocks(gate_x_weight), rate
    )


def body(
    tokens,
    ffn1_gain,
    ffn1_gate,
    ffn1_up,
    ffn1_down,
    mix_gain,
    lru_in_weight,
    lru_gate_weight,
    conv_weight,
    gate_a_weight,
    gate_x_weight,
    decay_param,
    mix_out_weight,
    ffn2_gain,
    ffn2_gate,
    ffn2_up,
    ffn2_down,
):
    ends = [((1, 640, HALF), (2, 640, HALF))]
    gates, uppers = full_tiles(1, 5), full_tiles(2, 5)
    downs = full_tiles(0, 5) + [((0, 640, HALF),)]
    order = gates + uppers + ends
    mixing = full_tiles(0, 1) + full_tiles(1, 1) + [((0, LANES, HALF), (1, LANES, HALF))]
    mixing += full_tiles(2, 1) + [((2, LANES, HALF),)]
    packed_mixing = gather_tiles(
        mixing, [lru_in_weight, lru_gate_weight, mix_out_weight.T]
    )
    packed = gather_tiles(downs + order, [ffn2_down.T, ffn2_gate, ffn2_up])

    own, others = packed_tiles(downs + order, [ffn1_down.T, ffn1_gate, ffn1_up], (8, 9), (1, 1))
    own = lax.all_gather(own, "y", axis=0)
    block, *far = spread_over_z(others)
    weights = spread_z_last(own, *far) + spread_over_y(block)

    normed = turned_norm(tokens, ffn1_gain)
    normed = after(normed, block)
    rows = gather_rows(normed)
    sums = sent_sums(ffn_terms(rows, first_ffn_kernel, weights))
    first, normed = combined(tokens, sums, True, "zy", mix_gain)
    rows = gather_rows(normed)
    sums = sent_sums(
        mixer_terms(rows, packed_mixing, conv_weight, gate_a_weight, gate_x_weight, decay_param),
    )
    second, normed = combined(first, sums, False, "", ffn2_gain)
    rows = gather_rows(normed)
    sums = sent_sums(ffn_terms(rows, ffn_kernel, [packed]))
    return combined(second, sums, True)[0]


def solution(mesh):
    split = Mesh(mesh.devices.reshape(8, 4, 4, 2), FS_TP)
    placed = (
        P(FS_TP, None),
        P(),
        P(FS, TP),
        P(FS, TP),
        P(TP, FS),
        P(),
        P(FS, TP),
        P(FS, TP),
        P(None, TP),
        P(TP, None, None),
        P(TP, None, None),
        P(TP),
        P(TP, FS),
        P(),
        P(FS, TP),
        P(FS, TP),
        P(TP, FS),
    )

    return jax.shard_map(
        body, mesh=split, in_specs=placed, out_specs=P(FS_TP, None), check_vma=False
    )
```

profile of v0, /device:TPU:1, one launch (start us, length us, event | category | flops | bytes accessed | tf_op | source)
XLA Modules:
  0.0 240.4 jit_solution(11688919382303359019)
XLA Ops:
  11.0 6.4 %collective-permute-start = (bf16[9,64,128]{2,1,0:T(8,128)(2,1)S(1)}, bf16[9,64,128]{2,1,0:T(8,128)(2,1)S(1)}, u32[]{:S(2)}, u32[]{:S(2)}) collective-permute-start(bf16[9,64,128]{2,1,0:T(8,128)(2,1)S(1)} %get-tuple-element.33.refs_0_), channel_id=1, source_target_pairs={{0,224},{32,0},{64,32},{96,64},{128,96},{160,128},{192,160},{224,1... | collective-permute-start | bytes 442376 | tf_op jit(solution)/shard_map/ppermute | solution.py:24
  20.0 3.1 %collective-permute-done.1.refs_7_ = bf16[9,64,128]{2,1,0:T(8,128)(2,1)S(1)} collective-permute-done((bf16[9,64,128]{2,1,0:T(8,128)(2,1)S(1)}, bf16[9,64,128]{2,1,0:T(8,128)(2,1)S(1)}, u32[]{:S(2)}, u32[]{:S(2)}) %collective-permute-start.1) | collective-permute-done | bytes 147488 | tf_op jit(solution)/shard_map/ppermute | solution.py:24
  30.1 11.0 %all-gather = bf16[32,64,128]{2,1,0:T(8,128)(2,1)S(1)} all-gather(bf16[8,64,128]{2,1,0:T(8,128)(2,1)S(1)} %get-tuple-element.41), channel_id=2, replica_groups=mesh['z'=8,'y'=4,'x'=4,'c'=2] {'y'}, dimensions={0}, use_global_device_ids=true | all-gather | bytes 655360 | tf_op jit(solution)/shard_map/all_gather | solution.py:445
  45.8 7.7 %collective-permute-done.6.refs_4_ = bf16[9,64,128]{2,1,0:T(8,128)(2,1)S(1)} collective-permute-done((bf16[9,64,128]{2,1,0:T(8,128)(2,1)S(1)}, bf16[9,64,128]{2,1,0:T(8,128)(2,1)S(1)}, u32[]{:S(2)}, u32[]{:S(2)}) %collective-permute-start.6) | collective-permute-done | bytes 147488 | tf_op jit(solution)/shard_map/ppermute | solution.py:24
  53.6 4.5 %collective-permute-start.15 = (bf16[8,9,64,128]{3,2,1,0:T(8,128)(2,1)S(1)}, bf16[8,9,64,128]{3,2,1,0:T(8,128)(2,1)S(1)}, u32[]{:S(2)}, u32[]{:S(2)}) collective-permute-start(bf16[8,9,64,128]{3,2,1,0:T(8,128)(2,1)S(1)} %shard_map.164.refs_8_), channel_id=1, source_target_pairs={{0,24},{8,0},{16,8},{24,16},{1,25},{9,1},{17,9},{25,17},{2,26},{10... | collective-permute-start | bytes 3538952 | tf_op jit(solution)/shard_map/ppermute | solution.py:24
  58.1 3.5 %collective-permute-start.10 = (bf16[4,8,64,128]{3,2,1,0:T(8,128)(2,1)S(1)}, bf16[4,8,64,128]{3,2,1,0:T(8,128)(2,1)S(1)}, u32[]{:S(2)}, u32[]{:S(2)}) collective-permute-start(bf16[4,8,64,128]{3,2,1,0:T(8,128)(2,1)S(1)} %collective-permute-done.8.refs_1_), channel_id=1, source_target_pairs={{0,224},{32,0},{64,32},{96,64},{128,96},{160,128},{192,160},{224,1... | collective-permute-start | bytes 1572872 | tf_op jit(solution)/shard_map/ppermute | solution.py:24
  62.0 11.1 %collective-permute-done.10.refs_2_ = bf16[4,8,64,128]{3,2,1,0:T(8,128)(2,1)S(1)} collective-permute-done((bf16[4,8,64,128]{3,2,1,0:T(8,128)(2,1)S(1)}, bf16[4,8,64,128]{3,2,1,0:T(8,128)(2,1)S(1)}, u32[]{:S(2)}, u32[]{:S(2)}) %collective-permute-start.10) | collective-permute-done | bytes 524320 | tf_op jit(solution)/shard_map/ppermute | solution.py:24
  73.1 3.4 %collective-permute-done.11.refs_6_ = bf16[4,8,64,128]{3,2,1,0:T(8,128)(2,1)S(1)} collective-permute-done((bf16[4,8,64,128]{3,2,1,0:T(8,128)(2,1)S(1)}, bf16[4,8,64,128]{3,2,1,0:T(8,128)(2,1)S(1)}, u32[]{:S(2)}, u32[]{:S(2)}) %collective-permute-start.11) | collective-permute-done | bytes 524320 | tf_op jit(solution)/shard_map/ppermute | solution.py:24
  78.0 11.5 %all_gather.21.mine_ref = bf16[192,2048]{1,0:T(8,128)(2,1)S(1)} all-gather(bf16[48,2048]{1,0:T(8,128)(2,1)S(1)} %shard_map.163), channel_id=1, replica_groups=mesh['z'=8,'y'=4,'x'=4,'c'=2] {'x'}, dimensions={0}, use_global_device_ids=true | all-gather | bytes 983040 | tf_op jit(solution)/shard_map/all_gather | solution.py:94
  89.5 11.0 %collective-permute-start.7 = (bf16[192,2048]{1,0:T(8,128)(2,1)S(1)}, bf16[192,2048]{1,0:T(8,128)(2,1)S(1)}, u32[]{:S(2)}, u32[]{:S(2)}) collective-permute-start(bf16[192,2048]{1,0:T(8,128)(2,1)S(1)} %all_gather.21.mine_ref), channel_id=1, source_target_pairs={{0,1},{1,0},{2,3},{3,2},{4,5},{5,4},{6,7},{7,6},{8,9},{9,8},{10,11... | collective-permute-start | bytes 2359304 | tf_op jit(solution)/shard_map/ppermute | solution.py:24
  100.6 5.5 %collective-permute-start.17 = (bf16[8,5,64,128]{3,2,1,0:T(8,128)(2,1)S(1)}, bf16[8,5,64,128]{3,2,1,0:T(8,128)(2,1)S(1)}, u32[]{:S(2)}, u32[]{:S(2)}) collective-permute-start(bf16[8,5,64,128]{3,2,1,0:T(8,128)(2,1)S(1)} %slice.24), channel_id=1, source_target_pairs={{0,24},{8,0},{16,8},{24,16},{1,25},{9,1},{17,9},{25,17},{2,26},{10... | collective-permute-start | bytes 1966088 | tf_op jit(solution)/shard_map/ppermute | solution.py:24
  107.2 16.4 %collective-permute-done.18.refs_11_ = bf16[8,4,64,128]{3,2,1,0:T(8,128)(2,1)S(1)} collective-permute-done((bf16[8,4,64,128]{3,2,1,0:T(8,128)(2,1)S(1)}, bf16[8,4,64,128]{3,2,1,0:T(8,128)(2,1)S(1)}, u32[]{:S(2)}, u32[]{:S(2)}) %collective-permute-start.18) | collective-permute-done | bytes 524320 | tf_op jit(solution)/shard_map/ppermute | solution.py:24
  124.0 3.8 %shard_map.165 = (bf16[192,2048]{1,0:T(8,128)(2,1)S(1)}, bf16[192,2048]{1,0:T(8,128)(2,1)S(1)}) custom-call(bf16[192,2048]{1,0:T(8,128)(2,1)S(1)} %all_gather.21.mine_ref, bf16[192,2048]{1,0:T(8,128)(2,1)S(1)} %collective-permute-done.7.other_ref, bf16[4,8,64,128]{3,2,1,0:T(8,128)(2,1)S(1)} %bitcast.36, ...), custom_call_target="tpu_custom_call" | custom-call | tf_op jit(solution)/shard_map/pallas_call | solution.py:37
  132.3 3.6 %all-to-all-start = ((bf16[4,48,2048]{2,1,0:T(8,128)(2,1)}), bf16[4,48,2048]{2,1,0:T(8,128)(2,1)S(1)}, u32[]{:S(2)}, u32[]{:S(2)}) async-start(bf16[4,48,2048]{2,1,0:T(8,128)(2,1)} %shard_map.166), calls=%async_computation | async-start | bytes 1572864 | tf_op jit(solution)/shard_map/all_to_all | solution.py:113
  136.1 11.9 %all-to-all-done.refs_1_ = bf16[4,48,2048]{2,1,0:T(8,128)(2,1)S(1)} async-done(((bf16[4,48,2048]{2,1,0:T(8,128)(2,1)}), bf16[4,48,2048]{2,1,0:T(8,128)(2,1)S(1)}, u32[]{:S(2)}, u32[]{:S(2)}) %all-to-all-start) | async-done | bytes 786464 | tf_op jit(solution)/shard_map/all_to_all | solution.py:113
  148.5 11.6 %all_gather.24.mine_ref = bf16[192,2048]{1,0:T(8,128)(2,1)S(1)} all-gather(bf16[48,2048]{1,0:T(8,128)(2,1)S(1)} %get-tuple-element.54), channel_id=1, replica_groups=mesh['z'=8,'y'=4,'x'=4,'c'=2] {'x'}, dimensions={0}, use_global_device_ids=true | all-gather | bytes 983040 | tf_op jit(solution)/shard_map/all_gather | solution.py:94
  160.1 3.7 %collective-permute-start.20 = (bf16[192,2048]{1,0:T(8,128)(2,1)S(1)}, bf16[192,2048]{1,0:T(8,128)(2,1)S(1)}, u32[]{:S(2)}, u32[]{:S(2)}) collective-permute-start(bf16[192,2048]{1,0:T(8,128)(2,1)S(1)} %all_gather.24.mine_ref), channel_id=1, source_target_pairs={{0,1},{1,0},{2,3},{3,2},{4,5},{5,4},{6,7},{7,6},{8,9},{9,8},{10,11... | collective-permute-start | bytes 2359304 | tf_op jit(solution)/shard_map/ppermute | solution.py:24
  167.5 4.7 %shard_map.168 = (bf16[192,2048]{1,0:T(8,128)(2,1)S(1)}, bf16[192,2048]{1,0:T(8,128)(2,1)S(1)}) custom-call(bf16[192,2048]{1,0:T(8,128)(2,1)S(1)} %all_gather.24.mine_ref, bf16[192,2048]{1,0:T(8,128)(2,1)S(1)} %collective-permute-done.20.other_ref, bf16[32,5,64,128]{3,2,1,0:T(8,128)(2,1)S(1)} %bitcast.33, f32[4,256]{1,0:T(4,128)S(1)} %pad_convert_fusion.taps_ref, ...), custom_call_target="tpu_custom_call" | custom-call | tf_op jit(solution)/shard_map/pallas_call | solution.py:37
  174.8 13.9 %all_to_all.15.refs_1_ = bf16[4,48,2048]{2,1,0:T(8,128)(2,1)S(1)} all-to-all(bf16[4,48,2048]{2,1,0:T(8,128)(2,1)S(1)} %shard_map.169), channel_id=1, replica_groups=mesh['z'=8,'y'=4,'x'=4,'c'=2] {'x'}, dimensions={0} | all-to-all | bytes 1572864 | tf_op jit(solution)/shard_map/all_to_all | solution.py:113
  188.9 11.5 %all_gather.26.mine_ref = bf16[192,2048]{1,0:T(8,128)(2,1)S(1)} all-gather(bf16[48,2048]{1,0:T(8,128)(2,1)S(1)} %get-tuple-element.58), channel_id=1, replica_groups=mesh['z'=8,'y'=4,'x'=4,'c'=2] {'x'}, dimensions={0}, use_global_device_ids=true | all-gather | bytes 983040 | tf_op jit(solution)/shard_map/all_gather | solution.py:94
  200.5 4.5 %collective-permute-start.22 = (bf16[192,2048]{1,0:T(8,128)(2,1)S(1)}, bf16[192,2048]{1,0:T(8,128)(2,1)S(1)}, u32[]{:S(2)}, u32[]{:S(2)}) collective-permute-start(bf16[192,2048]{1,0:T(8,128)(2,1)S(1)} %all_gather.26.mine_ref), channel_id=1, source_target_pairs={{0,1},{1,0},{2,3},{3,2},{4,5},{5,4},{6,7},{7,6},{8,9},{9,8},{10,11... | collective-permute-start | bytes 2359304 | tf_op jit(solution)/shard_map/ppermute | solution.py:24
  206.9 3.5 %copy-done = bf16[34816,128]{1,0:T(8,128)(2,1)S(1)} copy-done((bf16[34816,128]{1,0:T(8,128)(2,1)S(1)}, bf16[34816,128]{1,0:T(8,128)(2,1)}, u32[]{:S(2)}) %copy-start) | copy-done | bytes 8912920
  210.4 5.5 %shard_map.171 = (bf16[192,2048]{1,0:T(8,128)(2,1)S(1)}, bf16[192,2048]{1,0:T(8,128)(2,1)S(1)}) custom-call(bf16[192,2048]{1,0:T(8,128)(2,1)S(1)} %all_gather.26.mine_ref, bf16[192,2048]{1,0:T(8,128)(2,1)S(1)} %collective-permute-done.22.other_ref, bf16[32,17,64,128]{3,2,1,0:T(8,128)(2,1)S(1)} %bitcast.32), custom_call_target="tpu_custom_call" | custom-call | tf_op jit(solution)/shard_map/pallas_call | solution.py:37
  218.5 14.3 %all_to_all.16.refs_1_ = bf16[4,48,2048]{2,1,0:T(8,128)(2,1)S(1)} all-to-all(bf16[4,48,2048]{2,1,0:T(8,128)(2,1)S(1)} %shard_map.172), channel_id=1, replica_groups=mesh['z'=8,'y'=4,'x'=4,'c'=2] {'x'}, dimensions={0} | all-to-all | bytes 1572864 | tf_op jit(solution)/shard_map/all_to_all | solution.py:113
  (83 shorter events, 39.0 us)
Async XLA Ops:
  6.5 159.2 %all-gather.4.cloned.1.call-start = ((), (), s32[]{:S(2)}) async-start(), calls=%async_computation.3 | async-start | bytes 2703360 | tf_op jit(solution)/shard_map/all_gather | solution.py:176
  8.1 198.8 %all-gather.6.cloned.1.call-start = ((), (), s32[]{:S(2)}) async-start(), calls=%async_computation.4 | async-start | bytes 9191424 | tf_op jit(solution)/shard_map/all_gather | solution.py:176
  11.0 8.9 %collective-permute-start = (bf16[9,64,128]{2,1,0:T(8,128)(2,1)S(1)}, bf16[9,64,128]{2,1,0:T(8,128)(2,1)S(1)}, u32[]{:S(2)}, u32[]{:S(2)}) collective-permute-start(bf16[9,64,128]{2,1,0:T(8,128)(2,1)S(1)} %get-tuple-element.33.refs_0_), channel_id=1, source_target_pairs={{0,224},{32,0},{64,32},{96,64},{128,96},{160,128},{192,160},{224,1... | collective-permute-start | bytes 442376 | tf_op jit(solution)/shard_map/ppermute | solution.py:24
  17.4 5.7 %collective-permute-start.1 = (bf16[9,64,128]{2,1,0:T(8,128)(2,1)S(1)}, bf16[9,64,128]{2,1,0:T(8,128)(2,1)S(1)}, u32[]{:S(2)}, u32[]{:S(2)}) collective-permute-start(bf16[9,64,128]{2,1,0:T(8,128)(2,1)S(1)} %get-tuple-element.33.refs_0_), channel_id=1, source_target_pairs={{0,32},{32,64},{64,96},{96,128},{128,160},{160,192},{192,224},{224... | collective-permute-start | bytes 442376 | tf_op jit(solution)/shard_map/ppermute | solution.py:24
  23.1 4.0 %collective-permute-start.2 = (bf16[9,64,128]{2,1,0:T(8,128)(2,1)S(1)}, bf16[9,64,128]{2,1,0:T(8,128)(2,1)S(1)}, u32[]{:S(2)}, u32[]{:S(2)}) collective-permute-start(bf16[9,64,128]{2,1,0:T(8,128)(2,1)S(1)} %collective-permute-done.refs_1_), channel_id=1, source_target_pairs={{0,224},{32,0},{64,32},{96,64},{128,96},{160,128},{192,160},{224,1... | collective-permute-start | bytes 442376 | tf_op jit(solution)/shard_map/ppermute | solution.py:24
  23.4 5.2 %collective-permute-start.3 = (bf16[9,64,128]{2,1,0:T(8,128)(2,1)S(1)}, bf16[9,64,128]{2,1,0:T(8,128)(2,1)S(1)}, u32[]{:S(2)}, u32[]{:S(2)}) collective-permute-start(bf16[9,64,128]{2,1,0:T(8,128)(2,1)S(1)} %collective-permute-done.1.refs_7_), channel_id=1, source_target_pairs={{0,32},{32,64},{64,96},{96,128},{128,160},{160,192},{192,224},{224... | collective-permute-start | bytes 442376 | tf_op jit(solution)/shard_map/ppermute | solution.py:24
  28.6 12.5 %collective-permute-start.4 = (bf16[9,64,128]{2,1,0:T(8,128)(2,1)S(1)}, bf16[9,64,128]{2,1,0:T(8,128)(2,1)S(1)}, u32[]{:S(2)}, u32[]{:S(2)}) collective-permute-start(bf16[9,64,128]{2,1,0:T(8,128)(2,1)S(1)} %collective-permute-done.2.refs_2_), channel_id=1, source_target_pairs={{0,224},{32,0},{64,32},{96,64},{128,96},{160,128},{192,160},{224,1... | collective-permute-start | bytes 442376 | tf_op jit(solution)/shard_map/ppermute | solution.py:24
  28.6 12.5 %collective-permute-start.5 = (bf16[9,64,128]{2,1,0:T(8,128)(2,1)S(1)}, bf16[9,64,128]{2,1,0:T(8,128)(2,1)S(1)}, u32[]{:S(2)}, u32[]{:S(2)}) collective-permute-start(bf16[9,64,128]{2,1,0:T(8,128)(2,1)S(1)} %collective-permute-done.3.refs_6_), channel_id=1, source_target_pairs={{0,32},{32,64},{64,96},{96,128},{128,160},{160,192},{192,224},{224... | collective-permute-start | bytes 442376 | tf_op jit(solution)/shard_map/ppermute | solution.py:24
  41.1 17.0 %collective-permute-start.8 = (bf16[4,8,64,128]{3,2,1,0:T(8,128)(2,1)S(1)}, bf16[4,8,64,128]{3,2,1,0:T(8,128)(2,1)S(1)}, u32[]{:S(2)}, u32[]{:S(2)}) collective-permute-start(bf16[4,8,64,128]{3,2,1,0:T(8,128)(2,1)S(1)} %bitcast.34), channel_id=1, source_target_pairs={{0,224},{32,0},{64,32},{96,64},{128,96},{160,128},{192,160},{224,1... | collective-permute-start | bytes 1572872 | tf_op jit(solution)/shard_map/ppermute | solution.py:24
  43.2 14.9 %collective-permute-start.9 = (bf16[4,8,64,128]{3,2,1,0:T(8,128)(2,1)S(1)}, bf16[4,8,64,128]{3,2,1,0:T(8,128)(2,1)S(1)}, u32[]{:S(2)}, u32[]{:S(2)}) collective-permute-start(bf16[4,8,64,128]{3,2,1,0:T(8,128)(2,1)S(1)} %bitcast.35), channel_id=1, source_target_pairs={{0,32},{32,64},{64,96},{96,128},{128,160},{160,192},{192,224},{224... | collective-permute-start | bytes 1572872 | tf_op jit(solution)/shard_map/ppermute | solution.py:24
  43.2 10.4 %collective-permute-start.6 = (bf16[9,64,128]{2,1,0:T(8,128)(2,1)S(1)}, bf16[9,64,128]{2,1,0:T(8,128)(2,1)S(1)}, u32[]{:S(2)}, u32[]{:S(2)}) collective-permute-start(bf16[9,64,128]{2,1,0:T(8,128)(2,1)S(1)} %collective-permute-done.4.refs_3_), channel_id=1, source_target_pairs={{0,224},{32,0},{64,32},{96,64},{128,96},{160,128},{192,160},{224,1... | collective-permute-start | bytes 442376 | tf_op jit(solution)/shard_map/ppermute | solution.py:24
  53.6 46.9 %collective-permute-start.15 = (bf16[8,9,64,128]{3,2,1,0:T(8,128)(2,1)S(1)}, bf16[8,9,64,128]{3,2,1,0:T(8,128)(2,1)S(1)}, u32[]{:S(2)}, u32[]{:S(2)}) collective-permute-start(bf16[8,9,64,128]{3,2,1,0:T(8,128)(2,1)S(1)} %shard_map.164.refs_8_), channel_id=1, source_target_pairs={{0,24},{8,0},{16,8},{24,16},{1,25},{9,1},{17,9},{25,17},{2,26},{10... | collective-permute-start | bytes 3538952 | tf_op jit(solution)/shard_map/ppermute | solution.py:24
  58.1 42.4 %collective-permute-start.16 = (bf16[8,9,64,128]{3,2,1,0:T(8,128)(2,1)S(1)}, bf16[8,9,64,128]{3,2,1,0:T(8,128)(2,1)S(1)}, u32[]{:S(2)}, u32[]{:S(2)}) collective-permute-start(bf16[8,9,64,128]{3,2,1,0:T(8,128)(2,1)S(1)} %shard_map.164.refs_8_), channel_id=1, source_target_pairs={{0,8},{8,16},{16,24},{24,0},{1,9},{9,17},{17,25},{25,1},{2,10},{10... | collective-permute-start | bytes 3538952 | tf_op jit(solution)/shard_map/ppermute | solution.py:24
  58.1 15.0 %collective-permute-start.10 = (bf16[4,8,64,128]{3,2,1,0:T(8,128)(2,1)S(1)}, bf16[4,8,64,128]{3,2,1,0:T(8,128)(2,1)S(1)}, u32[]{:S(2)}, u32[]{:S(2)}) collective-permute-start(bf16[4,8,64,128]{3,2,1,0:T(8,128)(2,1)S(1)} %collective-permute-done.8.refs_1_), channel_id=1, source_target_pairs={{0,224},{32,0},{64,32},{96,64},{128,96},{160,128},{192,160},{224,1... | collective-permute-start | bytes 1572872 | tf_op jit(solution)/shard_map/ppermute | solution.py:24
  61.6 14.9 %collective-permute-start.11 = (bf16[4,8,64,128]{3,2,1,0:T(8,128)(2,1)S(1)}, bf16[4,8,64,128]{3,2,1,0:T(8,128)(2,1)S(1)}, u32[]{:S(2)}, u32[]{:S(2)}) collective-permute-start(bf16[4,8,64,128]{3,2,1,0:T(8,128)(2,1)S(1)} %collective-permute-done.9.refs_7_), channel_id=1, source_target_pairs={{0,32},{32,64},{64,96},{96,128},{128,160},{160,192},{192,224},{224... | collective-permute-start | bytes 1572872 | tf_op jit(solution)/shard_map/ppermute | solution.py:24
  76.5 29.7 %collective-permute-start.12 = (bf16[4,8,64,128]{3,2,1,0:T(8,128)(2,1)S(1)}, bf16[4,8,64,128]{3,2,1,0:T(8,128)(2,1)S(1)}, u32[]{:S(2)}, u32[]{:S(2)}) collective-permute-start(bf16[4,8,64,128]{3,2,1,0:T(8,128)(2,1)S(1)} %collective-permute-done.10.refs_2_), channel_id=1, source_target_pairs={{0,224},{32,0},{64,32},{96,64},{128,96},{160,128},{192,160},{224,1... | collective-permute-start | bytes 1572872 | tf_op jit(solution)/shard_map/ppermute | solution.py:24
  76.6 29.6 %collective-permute-start.13 = (bf16[4,8,64,128]{3,2,1,0:T(8,128)(2,1)S(1)}, bf16[4,8,64,128]{3,2,1,0:T(8,128)(2,1)S(1)}, u32[]{:S(2)}, u32[]{:S(2)}) collective-permute-start(bf16[4,8,64,128]{3,2,1,0:T(8,128)(2,1)S(1)} %collective-permute-done.11.refs_6_), channel_id=1, source_target_pairs={{0,32},{32,64},{64,96},{96,128},{128,160},{160,192},{192,224},{224... | collective-permute-start | bytes 1572872 | tf_op jit(solution)/shard_map/ppermute | solution.py:24
  89.5 17.7 %collective-permute-start.7 = (bf16[192,2048]{1,0:T(8,128)(2,1)S(1)}, bf16[192,2048]{1,0:T(8,128)(2,1)S(1)}, u32[]{:S(2)}, u32[]{:S(2)}) collective-permute-start(bf16[192,2048]{1,0:T(8,128)(2,1)S(1)} %all_gather.21.mine_ref), channel_id=1, source_target_pairs={{0,1},{1,0},{2,3},{3,2},{4,5},{5,4},{6,7},{7,6},{8,9},{9,8},{10,11... | collective-permute-start | bytes 2359304 | tf_op jit(solution)/shard_map/ppermute | solution.py:24
  100.6 23.1 %collective-permute-start.17 = (bf16[8,5,64,128]{3,2,1,0:T(8,128)(2,1)S(1)}, bf16[8,5,64,128]{3,2,1,0:T(8,128)(2,1)S(1)}, u32[]{:S(2)}, u32[]{:S(2)}) collective-permute-start(bf16[8,5,64,128]{3,2,1,0:T(8,128)(2,1)S(1)} %slice.24), channel_id=1, source_target_pairs={{0,24},{8,0},{16,8},{24,16},{1,25},{9,1},{17,9},{25,17},{2,26},{10... | collective-permute-start | bytes 1966088 | tf_op jit(solution)/shard_map/ppermute | solution.py:24
  106.1 17.6 %collective-permute-start.18 = (bf16[8,4,64,128]{3,2,1,0:T(8,128)(2,1)S(1)}, bf16[8,4,64,128]{3,2,1,0:T(8,128)(2,1)S(1)}, u32[]{:S(2)}, u32[]{:S(2)}) collective-permute-start(bf16[8,4,64,128]{3,2,1,0:T(8,128)(2,1)S(1)} %slice.25), channel_id=1, source_target_pairs={{0,8},{8,16},{16,24},{24,0},{1,9},{9,17},{17,25},{25,1},{2,10},{10... | collective-permute-start | bytes 1572872 | tf_op jit(solution)/shard_map/ppermute | solution.py:24
  106.2 17.8 %collective-permute-start.14 = (bf16[4,8,64,128]{3,2,1,0:T(8,128)(2,1)S(1)}, bf16[4,8,64,128]{3,2,1,0:T(8,128)(2,1)S(1)}, u32[]{:S(2)}, u32[]{:S(2)}) collective-permute-start(bf16[4,8,64,128]{3,2,1,0:T(8,128)(2,1)S(1)} %collective-permute-done.12.refs_3_), channel_id=1, source_target_pairs={{0,224},{32,0},{64,32},{96,64},{128,96},{160,128},{192,160},{224,1... | collective-permute-start | bytes 1572872 | tf_op jit(solution)/shard_map/ppermute | solution.py:24
  132.3 15.6 %all-to-all-start = ((bf16[4,48,2048]{2,1,0:T(8,128)(2,1)}), bf16[4,48,2048]{2,1,0:T(8,128)(2,1)S(1)}, u32[]{:S(2)}, u32[]{:S(2)}) async-start(bf16[4,48,2048]{2,1,0:T(8,128)(2,1)} %shard_map.166), calls=%async_computation | async-start | bytes 1572864 | tf_op jit(solution)/shard_map/all_to_all | solution.py:113
  160.1 5.6 %collective-permute-start.20 = (bf16[192,2048]{1,0:T(8,128)(2,1)S(1)}, bf16[192,2048]{1,0:T(8,128)(2,1)S(1)}, u32[]{:S(2)}, u32[]{:S(2)}) collective-permute-start(bf16[192,2048]{1,0:T(8,128)(2,1)S(1)} %all_gather.24.mine_ref), channel_id=1, source_target_pairs={{0,1},{1,0},{2,3},{3,2},{4,5},{5,4},{6,7},{7,6},{8,9},{9,8},{10,11... | collective-permute-start | bytes 2359304 | tf_op jit(solution)/shard_map/ppermute | solution.py:24
  200.5 6.4 %collective-permute-start.22 = (bf16[192,2048]{1,0:T(8,128)(2,1)S(1)}, bf16[192,2048]{1,0:T(8,128)(2,1)S(1)}, u32[]{:S(2)}, u32[]{:S(2)}) collective-permute-start(bf16[192,2048]{1,0:T(8,128)(2,1)S(1)} %all_gather.26.mine_ref), channel_id=1, source_target_pairs={{0,1},{1,0},{2,3},{3,2},{4,5},{5,4},{6,7},{7,6},{8,9},{9,8},{10,11... | collective-permute-start | bytes 2359304 | tf_op jit(solution)/shard_map/ppermute | solution.py:24
  (13 other events, 147.0 us)
Sparse Core Ops, SparseCore 0:
  9.9 85.8 all-gather.3
  98.4 98.7 all-gather.5
where the time goes:
time: 241 us; the launch traced here: 240 us
  blocking collectives  73.9 us (31%)
  waiting for transfers between devices  70.1 us (29%)
  starting transfers between devices  55.3 us (23%)
  Pallas kernels  21.9 us (9%)
  between operations  13.6 us (6%)
  local copies, waits for them, and re-layouts  5.45 us (2%)
    ppermute x24, waiting for transfers between devices, moved(): lax.ppermute(value, axis, [(i, (i - by) % count) for i in range(count)])  58.1 us
    ppermute x24, starting transfers between devices, moved(): lax.ppermute(value, axis, [(i, (i - by) % count) for i in range(count)])  51.6 us
    all_gather x3, blocking collectives, gather_rows(): mine = lax.all_gather(own, 'x', axis=0, tiled=True)  34.7 us
    all_to_all x2, blocking collectives, sent_sums(): return lax.all_to_all(sums, 'x', split_axis=0, concat_axis=0, tiled=True)  28.2 us
    pallas_call x11, Pallas kernels, call(): pl.pallas_call(kernel, in_specs=vmem_specs(len(args)), out_specs=jax.tree...  17.5 us
    all_to_all x1, waiting for transfers between devices, sent_sums(): return lax.all_to_all(sums, 'x', split_axis=0, concat_axis=0, tiled=True)  11.9 us
    all_gather x1, blocking collectives, body(): own = lax.all_gather(own, 'y', axis=0)  11 us
    unnamed x20, local copies, waits for them, and re-layouts  5.35 us
  transfers between devices with their start and end apart: 27, of which 15 were waited for; matrix products, arithmetic and copies ran while one was open for 0% of the time, Pallas kernels for 6%

commit v1 on v0

--- a/solution.py
+++ b/solution.py
@@ -15,7 +15,7 @@
 SHARD = 64
 HALF = 64
 WIDE = 256
-FFN_LOOPED = (False, True)
+FFN_LOOPED = (False, False)
 PARAMS = pltpu.CompilerParams(vmem_limit_bytes=24 << 20)
 
 
@@ -110,13 +110,34 @@
     out = pltpu.VMEM((count, mine.shape[0] // count, mine.shape[1]), jnp.bfloat16)
     other = moved(other, "c", 1)
     sums = vmem_call(pair_sum_kernel, out)(mine, other)
-    return lax.all_to_all(sums, "x", split_axis=0, concat_axis=0, tiled=True)
-
-
-def combine_kernel(half, turned, turn, base_ref, sums_ref, *refs):
-    total = sums_ref[0].astype(jnp.float32)
-    for n in range(1, sums_ref.shape[0]):
-        total = total + sums_ref[n].astype(jnp.float32)
+    return [lax.all_to_all(sums, "x", split_axis=0, concat_axis=0, tiled=True)]
+
+
+def apart_kernel(mine_ref, other_ref, *out_refs):
+    rows, chips = out_refs[0].shape[0], len(out_refs)
+    for n, out_ref in enumerate(out_refs):
+        chip = lax.rem(lax.axis_index("x") + n, chips)
+        own = pl.ds(pl.multiple_of(chip * rows, rows), rows)
+        out_ref[...] = (
+            mine_ref[own].astype(jnp.float32) + other_ref[own].astype(jnp.float32)
+        ).astype(jnp.bfloat16)
+
+
+def last_sums(terms):
+    mine, other = terms
+    count = lax.axis_size("x")
+    outs = [pltpu.VMEM((mine.shape[0] // count, mine.shape[1]), jnp.bfloat16)] * count
+    sums = vmem_call(apart_kernel, outs)(mine, moved(other, "c", 1))
+    return [sums[0]] + [moved(sums[n], "x", -n) for n in range(1, count)]
+
+
+def combine_kernel(half, turned, turn, parts, base_ref, *refs):
+    sums, refs = refs[:parts], refs[parts:]
+    if parts == 1:
+        sums = [sums[0].at[n] for n in range(sums[0].shape[0])]
+    total = sums[0][...].astype(jnp.float32)
+    for part_ref in sums[1:]:
+        total = total + part_ref[...].astype(jnp.float32)
     total = turned_back(total, turned)
     if half:
         total = 0.5 * total
@@ -133,8 +154,8 @@
     shape = pltpu.VMEM(base.shape, jnp.bfloat16)
     extra = () if gain is None else (gain[None],)
     outs = [shape] * 2 if extra else [jax.ShapeDtypeStruct(base.shape, jnp.bfloat16)]
-    kernel = lambda *refs: combine_kernel(half, turned, turn, *refs)
-    return vmem_call(kernel, outs)(base, sums, *extra)
+    kernel = lambda *refs: combine_kernel(half, turned, turn, len(sums), *refs)
+    return vmem_call(kernel, outs)(base, *sums, *extra)
 
 
 def pack_kernel(plan, out_copies, counts, *refs):
@@ -171,10 +192,9 @@
     )(*[in_hbm(a) for a in arrays])
 
 
-def gather_tiles(plan, arrays):
-    (packed,) = packed_tiles(plan, arrays, (len(plan),), (1,))
+def gather_tiles(packed):
     full = lax.all_gather(packed.reshape(-1, LANES), FS, axis=0, tiled=True)
-    return full.reshape(-1, len(plan), SHARD, LANES)
+    return full.reshape(-1, *packed.shape)
 
 
 def full_tiles(which, count):
@@ -434,14 +454,21 @@
     gates, uppers = full_tiles(1, 5), full_tiles(2, 5)
     downs = full_tiles(0, 5) + [((0, 640, HALF),)]
     order = gates + uppers + ends
-    mixing = full_tiles(0, 1) + full_tiles(1, 1) + [((0, LANES, HALF), (1, LANES, HALF))]
-    mixing += full_tiles(2, 1) + [((2, LANES, HALF),)]
-    packed_mixing = gather_tiles(
-        mixing, [lru_in_weight, lru_gate_weight, mix_out_weight.T]
-    )
-    packed = gather_tiles(downs + order, [ffn2_down.T, ffn2_gate, ffn2_up])
-
-    own, others = packed_tiles(downs + order, [ffn1_down.T, ffn1_gate, ffn1_up], (8, 9), (1, 1))
+    mixing = full_tiles(3, 1) + full_tiles(4, 1) + [((3, LANES, HALF), (4, LANES, HALF))]
+    mixing += full_tiles(5, 1) + [((5, LANES, HALF),)]
+    from_two = [tuple((which + 6, at, size) for which, at, size in p) for p in downs + order]
+    own, others, mixing, second = packed_tiles(
+        downs + order + mixing + from_two,
+        [
+            *(ffn1_down.T, ffn1_gate, ffn1_up),
+            *(lru_in_weight, lru_gate_weight, mix_out_weight.T),
+            *(ffn2_down.T, ffn2_gate, ffn2_up),
+        ],
+        (8, 9, 5, 17),
+        (1, 1, 1, 1),
+    )
+    packed_mixing = gather_tiles(mixing)
+    packed = gather_tiles(second)
     own = lax.all_gather(own, "y", axis=0)
     block, *far = spread_over_z(others)
     weights = spread_z_last(own, *far) + spread_over_y(block)
@@ -451,13 +478,15 @@
     rows = gather_rows(normed)
     sums = sent_sums(ffn_terms(rows, first_ffn_kernel, weights))
     first, normed = combined(tokens, sums, True, "zy", mix_gain)
+    (packed_mixing,) = in_vmem(packed_mixing)
+    normed, packed_mixing = lax.optimization_barrier((normed, packed_mixing))
     rows = gather_rows(normed)
     sums = sent_sums(
         mixer_terms(rows, packed_mixing, conv_weight, gate_a_weight, gate_x_weight, decay_param),
     )
     second, normed = combined(first, sums, False, "", ffn2_gain)
     rows = gather_rows(normed)
-    sums = sent_sums(ffn_terms(rows, ffn_kernel, [packed]))
+    sums = last_sums(ffn_terms(rows, ffn_kernel, [packed]))
     return combined(second, sums, True)[0]
 
 

time: 241 us -> 233 us (0.967)
  blocking collectives: 73.9 us -> 60.7 us
  waiting for transfers between devices: 70.1 us -> 77.8 us
  Pallas kernels: 21.9 us -> 17.9 us
    all_to_all x2 -> x1, blocking collectives: 28.2 us -> 14 us  [sent_sums(): return [lax.all_to_all(sums, 'x', split_axis=0, concat_axis=0, tiled=True)]]
    ppermute x24 -> x27, waiting for transfers between devices: 58.1 us -> 65.3 us  [moved(): lax.ppermute(value, axis, [(i, (i - by) % count) for i in range(count)])]
    ppermute x24 -> x27, starting transfers between devices: 51.6 us -> 52.9 us  [moved(): lax.ppermute(value, axis, [(i, (i - by) % count) for i in range(count)])]
  transfers between devices with their start and end apart: 27 -> 30, of which waited for: 15 -> 17; matrix products, arithmetic and copies ran while one was open for 0% -> 0% of each run, Pallas kernels for 6% -> 5%
where the time goes in v1:
time: 233 us; the launch traced here: 232 us
  waiting for transfers between devices  77.8 us (33%)
  blocking collectives  60.7 us (26%)
  starting transfers between devices  56.6 us (24%)
  Pallas kernels  17.9 us (8%)
  between operations  13.6 us (6%)
  local copies, waits for them, and re-layouts  5.41 us (2%)
    ppermute x27, waiting for transfers between devices, moved(): lax.ppermute(value, axis, [(i, (i - by) % count) for i in range(count)])  65.3 us
    ppermute x27, starting transfers between devices, moved(): lax.ppermute(value, axis, [(i, (i - by) % count) for i in range(count)])  52.9 us
    all_gather x3, blocking collectives, gather_rows(): mine = lax.all_gather(own, 'x', axis=0, tiled=True)  35.3 us
    pallas_call x11, Pallas kernels, call(): pl.pallas_call(kernel, in_specs=vmem_specs(len(args)), out_specs=jax.tree...  15.9 us
    all_to_all x1, blocking collectives, sent_sums(): return [lax.all_to_all(sums, 'x', split_axis=0, concat_axis=0, tiled=True)]  14 us
    all_to_all x1, waiting for transfers between devices, sent_sums(): return [lax.all_to_all(sums, 'x', split_axis=0, concat_axis=0, tiled=True)]  11.7 us
    all_gather x1, blocking collectives, body(): own = lax.all_gather(own, 'y', axis=0)  11.4 us
    unnamed x20, local copies, waits for them, and re-layouts  5.31 us
  transfers between devices with their start and end apart: 30, of which 17 were waited for; matrix products, arithmetic and copies ran while one was open for 0% of the time, Pallas kernels for 5%

profile of v1, /device:TPU:1, one launch (start us, length us, event | category | flops | bytes accessed | tf_op | source)
XLA Modules:
  0.0 232.2 jit_solution(13956956409414247437)
XLA Ops:
  9.4 6.5 %collective-permute-start = (bf16[9,64,128]{2,1,0:T(8,128)(2,1)S(1)}, bf16[9,64,128]{2,1,0:T(8,128)(2,1)S(1)}, u32[]{:S(2)}, u32[]{:S(2)}) collective-permute-start(bf16[9,64,128]{2,1,0:T(8,128)(2,1)S(1)} %get-tuple-element.41.refs_0_), channel_id=1, source_target_pairs={{0,224},{32,0},{64,32},{96,64},{128,96},{160,128},{192,160},{224,1... | collective-permute-start | bytes 442376 | tf_op jit(solution)/shard_map/ppermute | solution.py:24
  18.4 3.1 %collective-permute-done.1.refs_7_ = bf16[9,64,128]{2,1,0:T(8,128)(2,1)S(1)} collective-permute-done((bf16[9,64,128]{2,1,0:T(8,128)(2,1)S(1)}, bf16[9,64,128]{2,1,0:T(8,128)(2,1)S(1)}, u32[]{:S(2)}, u32[]{:S(2)}) %collective-permute-start.1) | collective-permute-done | bytes 147488 | tf_op jit(solution)/shard_map/ppermute | solution.py:24
  28.5 11.4 %all-gather = bf16[32,64,128]{2,1,0:T(8,128)(2,1)S(1)} all-gather(bf16[8,64,128]{2,1,0:T(8,128)(2,1)S(1)} %get-tuple-element.49), channel_id=2, replica_groups=mesh['z'=8,'y'=4,'x'=4,'c'=2] {'y'}, dimensions={0}, use_global_device_ids=true | all-gather | bytes 655360 | tf_op jit(solution)/shard_map/all_gather | solution.py:472
  44.1 8.9 %collective-permute-done.6.refs_4_ = bf16[9,64,128]{2,1,0:T(8,128)(2,1)S(1)} collective-permute-done((bf16[9,64,128]{2,1,0:T(8,128)(2,1)S(1)}, bf16[9,64,128]{2,1,0:T(8,128)(2,1)S(1)}, u32[]{:S(2)}, u32[]{:S(2)}) %collective-permute-start.6) | collective-permute-done | bytes 147488 | tf_op jit(solution)/shard_map/ppermute | solution.py:24
  53.1 3.1 %collective-permute-start.15 = (bf16[8,9,64,128]{3,2,1,0:T(8,128)(2,1)S(1)}, bf16[8,9,64,128]{3,2,1,0:T(8,128)(2,1)S(1)}, u32[]{:S(2)}, u32[]{:S(2)}) collective-permute-start(bf16[8,9,64,128]{3,2,1,0:T(8,128)(2,1)S(1)} %shard_map.164.refs_8_), channel_id=1, source_target_pairs={{0,24},{8,0},{16,8},{24,16},{1,25},{9,1},{17,9},{25,17},{2,26},{10... | collective-permute-start | bytes 3538952 | tf_op jit(solution)/shard_map/ppermute | solution.py:24
  56.2 3.5 %collective-permute-start.10 = (bf16[4,8,64,128]{3,2,1,0:T(8,128)(2,1)S(1)}, bf16[4,8,64,128]{3,2,1,0:T(8,128)(2,1)S(1)}, u32[]{:S(2)}, u32[]{:S(2)}) collective-permute-start(bf16[4,8,64,128]{3,2,1,0:T(8,128)(2,1)S(1)} %collective-permute-done.8.refs_1_), channel_id=1, source_target_pairs={{0,224},{32,0},{64,32},{96,64},{128,96},{160,128},{192,160},{224,1... | collective-permute-start | bytes 1572872 | tf_op jit(solution)/shard_map/ppermute | solution.py:24
  60.1 9.8 %collective-permute-done.10.refs_2_ = bf16[4,8,64,128]{3,2,1,0:T(8,128)(2,1)S(1)} collective-permute-done((bf16[4,8,64,128]{3,2,1,0:T(8,128)(2,1)S(1)}, bf16[4,8,64,128]{3,2,1,0:T(8,128)(2,1)S(1)}, u32[]{:S(2)}, u32[]{:S(2)}) %collective-permute-start.10) | collective-permute-done | bytes 524320 | tf_op jit(solution)/shard_map/ppermute | solution.py:24
  69.9 3.0 %collective-permute-done.11.refs_6_ = bf16[4,8,64,128]{3,2,1,0:T(8,128)(2,1)S(1)} collective-permute-done((bf16[4,8,64,128]{3,2,1,0:T(8,128)(2,1)S(1)}, bf16[4,8,64,128]{3,2,1,0:T(8,128)(2,1)S(1)}, u32[]{:S(2)}, u32[]{:S(2)}) %collective-permute-start.11) | collective-permute-done | bytes 524320 | tf_op jit(solution)/shard_map/ppermute | solution.py:24
  74.3 11.8 %all_gather.21.mine_ref = bf16[192,2048]{1,0:T(8,128)(2,1)S(1)} all-gather(bf16[48,2048]{1,0:T(8,128)(2,1)S(1)} %shard_map.163), channel_id=1, replica_groups=mesh['z'=8,'y'=4,'x'=4,'c'=2] {'x'}, dimensions={0}, use_global_device_ids=true | all-gather | bytes 983040 | tf_op jit(solution)/shard_map/all_gather | solution.py:94
  86.2 9.9 %collective-permute-start.7 = (bf16[192,2048]{1,0:T(8,128)(2,1)S(1)}, bf16[192,2048]{1,0:T(8,128)(2,1)S(1)}, u32[]{:S(2)}, u32[]{:S(2)}) collective-permute-start(bf16[192,2048]{1,0:T(8,128)(2,1)S(1)} %all_gather.21.mine_ref), channel_id=1, source_target_pairs={{0,1},{1,0},{2,3},{3,2},{4,5},{5,4},{6,7},{7,6},{8,9},{9,8},{10,11... | collective-permute-start | bytes 2359304 | tf_op jit(solution)/shard_map/ppermute | solution.py:24
  96.2 6.1 %collective-permute-start.17 = (bf16[8,5,64,128]{3,2,1,0:T(8,128)(2,1)S(1)}, bf16[8,5,64,128]{3,2,1,0:T(8,128)(2,1)S(1)}, u32[]{:S(2)}, u32[]{:S(2)}) collective-permute-start(bf16[8,5,64,128]{3,2,1,0:T(8,128)(2,1)S(1)} %slice.24), channel_id=1, source_target_pairs={{0,24},{8,0},{16,8},{24,16},{1,25},{9,1},{17,9},{25,17},{2,26},{10... | collective-permute-start | bytes 1966088 | tf_op jit(solution)/shard_map/ppermute | solution.py:24
  103.5 15.5 %collective-permute-done.18.refs_11_ = bf16[8,4,64,128]{3,2,1,0:T(8,128)(2,1)S(1)} collective-permute-done((bf16[8,4,64,128]{3,2,1,0:T(8,128)(2,1)S(1)}, bf16[8,4,64,128]{3,2,1,0:T(8,128)(2,1)S(1)}, u32[]{:S(2)}, u32[]{:S(2)}) %collective-permute-start.18) | collective-permute-done | bytes 524320 | tf_op jit(solution)/shard_map/ppermute | solution.py:24
  119.4 3.8 %shard_map.165 = (bf16[192,2048]{1,0:T(8,128)(2,1)S(1)}, bf16[192,2048]{1,0:T(8,128)(2,1)S(1)}) custom-call(bf16[192,2048]{1,0:T(8,128)(2,1)S(1)} %all_gather.21.mine_ref, bf16[192,2048]{1,0:T(8,128)(2,1)S(1)} %collective-permute-done.7.other_ref, bf16[4,8,64,128]{3,2,1,0:T(8,128)(2,1)S(1)} %bitcast.36, ...), custom_call_target="tpu_custom_call" | custom-call | tf_op jit(solution)/shard_map/pallas_call | solution.py:37
  127.9 3.6 %all-to-all-start = ((bf16[4,48,2048]{2,1,0:T(8,128)(2,1)}), bf16[4,48,2048]{2,1,0:T(8,128)(2,1)S(1)}, u32[]{:S(2)}, u32[]{:S(2)}) async-start(bf16[4,48,2048]{2,1,0:T(8,128)(2,1)} %shard_map.166), calls=%async_computation | async-start | bytes 1572864 | tf_op jit(solution)/shard_map/all_to_all | solution.py:113
  131.6 11.7 %all-to-all-done.refs_1_ = bf16[4,48,2048]{2,1,0:T(8,128)(2,1)S(1)} async-done(((bf16[4,48,2048]{2,1,0:T(8,128)(2,1)}), bf16[4,48,2048]{2,1,0:T(8,128)(2,1)S(1)}, u32[]{:S(2)}, u32[]{:S(2)}) %all-to-all-start) | async-done | bytes 786464 | tf_op jit(solution)/shard_map/all_to_all | solution.py:113
  143.9 11.6 %all_gather.25.mine_ref = bf16[192,2048]{1,0:T(8,128)(2,1)S(1)} all-gather(bf16[48,2048]{1,0:T(8,128)(2,1)S(1)} %get-tuple-element.64), channel_id=1, replica_groups=mesh['z'=8,'y'=4,'x'=4,'c'=2] {'x'}, dimensions={0}, use_global_device_ids=true | all-gather | bytes 983040 | tf_op jit(solution)/shard_map/all_gather | solution.py:94
  155.5 4.2 %collective-permute-start.20 = (bf16[192,2048]{1,0:T(8,128)(2,1)S(1)}, bf16[192,2048]{1,0:T(8,128)(2,1)S(1)}, u32[]{:S(2)}, u32[]{:S(2)}) collective-permute-start(bf16[192,2048]{1,0:T(8,128)(2,1)S(1)} %all_gather.25.mine_ref), channel_id=1, source_target_pairs={{0,1},{1,0},{2,3},{3,2},{4,5},{5,4},{6,7},{7,6},{8,9},{9,8},{10,11... | collective-permute-start | bytes 2359304 | tf_op jit(solution)/shard_map/ppermute | solution.py:24
  163.3 4.7 %shard_map.168 = (bf16[192,2048]{1,0:T(8,128)(2,1)S(1)}, bf16[192,2048]{1,0:T(8,128)(2,1)S(1)}) custom-call(bf16[192,2048]{1,0:T(8,128)(2,1)S(1)} %all_gather.25.mine_ref, bf16[192,2048]{1,0:T(8,128)(2,1)S(1)} %collective-permute-done.20.other_ref, bf16[32,5,64,128]{3,2,1,0:T(8,128)(2,1)S(1)} %bitcast.33, f32[4,256]{1,0:T(4,128)S(1)} %pad_convert_fusion.taps_ref, ...), custom_call_target="tpu_custom_call" | custom-call | tf_op jit(solution)/shard_map/pallas_call | solution.py:37
  170.6 14.0 %all_to_all.10.refs_1_ = bf16[4,48,2048]{2,1,0:T(8,128)(2,1)S(1)} all-to-all(bf16[4,48,2048]{2,1,0:T(8,128)(2,1)S(1)} %shard_map.169), channel_id=1, replica_groups=mesh['z'=8,'y'=4,'x'=4,'c'=2] {'x'}, dimensions={0} | all-to-all | bytes 1572864 | tf_op jit(solution)/shard_map/all_to_all | solution.py:113
  184.8 11.8 %all_gather.26.mine_ref = bf16[192,2048]{1,0:T(8,128)(2,1)S(1)} all-gather(bf16[48,2048]{1,0:T(8,128)(2,1)S(1)} %get-tuple-element.69), channel_id=1, replica_groups=mesh['z'=8,'y'=4,'x'=4,'c'=2] {'x'}, dimensions={0}, use_global_device_ids=true | all-gather | bytes 983040 | tf_op jit(solution)/shard_map/all_gather | solution.py:94
  196.7 4.1 %collective-permute-start.22 = (bf16[192,2048]{1,0:T(8,128)(2,1)S(1)}, bf16[192,2048]{1,0:T(8,128)(2,1)S(1)}, u32[]{:S(2)}, u32[]{:S(2)}) collective-permute-start(bf16[192,2048]{1,0:T(8,128)(2,1)S(1)} %all_gather.26.mine_ref), channel_id=1, source_target_pairs={{0,1},{1,0},{2,3},{3,2},{4,5},{5,4},{6,7},{7,6},{8,9},{9,8},{10,11... | collective-permute-start | bytes 2359304 | tf_op jit(solution)/shard_map/ppermute | solution.py:24
  202.7 3.5 %copy-done = bf16[34816,128]{1,0:T(8,128)(2,1)S(1)} copy-done((bf16[34816,128]{1,0:T(8,128)(2,1)S(1)}, bf16[34816,128]{1,0:T(8,128)(2,1)}, u32[]{:S(2)}) %copy-start) | copy-done | bytes 8912920
  206.2 3.8 %shard_map.171 = (bf16[192,2048]{1,0:T(8,128)(2,1)S(1)}, bf16[192,2048]{1,0:T(8,128)(2,1)S(1)}) custom-call(bf16[192,2048]{1,0:T(8,128)(2,1)S(1)} %all_gather.26.mine_ref, bf16[192,2048]{1,0:T(8,128)(2,1)S(1)} %collective-permute-done.22.other_ref, bf16[32,17,64,128]{3,2,1,0:T(8,128)(2,1)S(1)} %bitcast.32), custom_call_target="tpu_custom_call" | custom-call | tf_op jit(solution)/shard_map/pallas_call | solution.py:37
  215.9 8.3 %collective-permute-done.24.refs_2_ = bf16[48,2048]{1,0:T(8,128)(2,1)S(1)} collective-permute-done((bf16[48,2048]{1,0:T(8,128)(2,1)S(1)}, bf16[48,2048]{1,0:T(8,128)(2,1)S(1)}, u32[]{:S(2)}, u32[]{:S(2)}) %collective-permute-start.24) | collective-permute-done | bytes 196640 | tf_op jit(solution)/shard_map/ppermute | solution.py:24
  (86 shorter events, 40.6 us)
Async XLA Ops:
  6.5 137.3 %all-gather.4.cloned.1.call-start = ((), (), s32[]{:S(2)}) async-start(), calls=%async_computation.2 | async-start | bytes 2703360 | tf_op jit(solution)/shard_map/all_gather | solution.py:196
  8.6 194.1 %all-gather.6.cloned.1.call-start = ((), (), s32[]{:S(2)}) async-start(), calls=%async_computation.3 | async-start | bytes 9191424 | tf_op jit(solution)/shard_map/all_gather | solution.py:196
  9.4 9.0 %collective-permute-start = (bf16[9,64,128]{2,1,0:T(8,128)(2,1)S(1)}, bf16[9,64,128]{2,1,0:T(8,128)(2,1)S(1)}, u32[]{:S(2)}, u32[]{:S(2)}) collective-permute-start(bf16[9,64,128]{2,1,0:T(8,128)(2,1)S(1)} %get-tuple-element.41.refs_0_), channel_id=1, source_target_pairs={{0,224},{32,0},{64,32},{96,64},{128,96},{160,128},{192,160},{224,1... | collective-permute-start | bytes 442376 | tf_op jit(solution)/shard_map/ppermute | solution.py:24
  27.0 12.9 %collective-permute-start.4 = (bf16[9,64,128]{2,1,0:T(8,128)(2,1)S(1)}, bf16[9,64,128]{2,1,0:T(8,128)(2,1)S(1)}, u32[]{:S(2)}, u32[]{:S(2)}) collective-permute-start(bf16[9,64,128]{2,1,0:T(8,128)(2,1)S(1)} %collective-permute-done.2.refs_2_), channel_id=1, source_target_pairs={{0,224},{32,0},{64,32},{96,64},{128,96},{160,128},{192,160},{224,1... | collective-permute-start | bytes 442376 | tf_op jit(solution)/shard_map/ppermute | solution.py:24
  27.0 12.9 %collective-permute-start.5 = (bf16[9,64,128]{2,1,0:T(8,128)(2,1)S(1)}, bf16[9,64,128]{2,1,0:T(8,128)(2,1)S(1)}, u32[]{:S(2)}, u32[]{:S(2)}) collective-permute-start(bf16[9,64,128]{2,1,0:T(8,128)(2,1)S(1)} %collective-permute-done.3.refs_6_), channel_id=1, source_target_pairs={{0,32},{32,64},{64,96},{96,128},{128,160},{160,192},{192,224},{224... | collective-permute-start | bytes 442376 | tf_op jit(solution)/shard_map/ppermute | solution.py:24
  39.9 16.2 %collective-permute-start.8 = (bf16[4,8,64,128]{3,2,1,0:T(8,128)(2,1)S(1)}, bf16[4,8,64,128]{3,2,1,0:T(8,128)(2,1)S(1)}, u32[]{:S(2)}, u32[]{:S(2)}) collective-permute-start(bf16[4,8,64,128]{3,2,1,0:T(8,128)(2,1)S(1)} %bitcast.34), channel_id=1, source_target_pairs={{0,224},{32,0},{64,32},{96,64},{128,96},{160,128},{192,160},{224,1... | collective-permute-start | bytes 1572872 | tf_op jit(solution)/shard_map/ppermute | solution.py:24
  41.4 14.8 %collective-permute-start.9 = (bf16[4,8,64,128]{3,2,1,0:T(8,128)(2,1)S(1)}, bf16[4,8,64,128]{3,2,1,0:T(8,128)(2,1)S(1)}, u32[]{:S(2)}, u32[]{:S(2)}) collective-permute-start(bf16[4,8,64,128]{3,2,1,0:T(8,128)(2,1)S(1)} %bitcast.35), channel_id=1, source_target_pairs={{0,32},{32,64},{64,96},{96,128},{128,160},{160,192},{192,224},{224... | collective-permute-start | bytes 1572872 | tf_op jit(solution)/shard_map/ppermute | solution.py:24
  41.5 11.5 %collective-permute-start.6 = (bf16[9,64,128]{2,1,0:T(8,128)(2,1)S(1)}, bf16[9,64,128]{2,1,0:T(8,128)(2,1)S(1)}, u32[]{:S(2)}, u32[]{:S(2)}) collective-permute-start(bf16[9,64,128]{2,1,0:T(8,128)(2,1)S(1)} %collective-permute-done.4.refs_3_), channel_id=1, source_target_pairs={{0,224},{32,0},{64,32},{96,64},{128,96},{160,128},{192,160},{224,1... | collective-permute-start | bytes 442376 | tf_op jit(solution)/shard_map/ppermute | solution.py:24
  53.1 43.0 %collective-permute-start.15 = (bf16[8,9,64,128]{3,2,1,0:T(8,128)(2,1)S(1)}, bf16[8,9,64,128]{3,2,1,0:T(8,128)(2,1)S(1)}, u32[]{:S(2)}, u32[]{:S(2)}) collective-permute-start(bf16[8,9,64,128]{3,2,1,0:T(8,128)(2,1)S(1)} %shard_map.164.refs_8_), channel_id=1, source_target_pairs={{0,24},{8,0},{16,8},{24,16},{1,25},{9,1},{17,9},{25,17},{2,26},{10... | collective-permute-start | bytes 3538952 | tf_op jit(solution)/shard_map/ppermute | solution.py:24
  56.1 40.0 %collective-permute-start.16 = (bf16[8,9,64,128]{3,2,1,0:T(8,128)(2,1)S(1)}, bf16[8,9,64,128]{3,2,1,0:T(8,128)(2,1)S(1)}, u32[]{:S(2)}, u32[]{:S(2)}) collective-permute-start(bf16[8,9,64,128]{3,2,1,0:T(8,128)(2,1)S(1)} %shard_map.164.refs_8_), channel_id=1, source_target_pairs={{0,8},{8,16},{16,24},{24,0},{1,9},{9,17},{17,25},{25,1},{2,10},{10... | collective-permute-start | bytes 3538952 | tf_op jit(solution)/shard_map/ppermute | solution.py:24
  56.2 13.7 %collective-permute-start.10 = (bf16[4,8,64,128]{3,2,1,0:T(8,128)(2,1)S(1)}, bf16[4,8,64,128]{3,2,1,0:T(8,128)(2,1)S(1)}, u32[]{:S(2)}, u32[]{:S(2)}) collective-permute-start(bf16[4,8,64,128]{3,2,1,0:T(8,128)(2,1)S(1)} %collective-permute-done.8.refs_1_), channel_id=1, source_target_pairs={{0,224},{32,0},{64,32},{96,64},{128,96},{160,128},{192,160},{224,1... | collective-permute-start | bytes 1572872 | tf_op jit(solution)/shard_map/ppermute | solution.py:24
  59.6 13.2 %collective-permute-start.11 = (bf16[4,8,64,128]{3,2,1,0:T(8,128)(2,1)S(1)}, bf16[4,8,64,128]{3,2,1,0:T(8,128)(2,1)S(1)}, u32[]{:S(2)}, u32[]{:S(2)}) collective-permute-start(bf16[4,8,64,128]{3,2,1,0:T(8,128)(2,1)S(1)} %collective-permute-done.9.refs_7_), channel_id=1, source_target_pairs={{0,32},{32,64},{64,96},{96,128},{128,160},{160,192},{192,224},{224... | collective-permute-start | bytes 1572872 | tf_op jit(solution)/shard_map/ppermute | solution.py:24
  72.9 29.6 %collective-permute-start.12 = (bf16[4,8,64,128]{3,2,1,0:T(8,128)(2,1)S(1)}, bf16[4,8,64,128]{3,2,1,0:T(8,128)(2,1)S(1)}, u32[]{:S(2)}, u32[]{:S(2)}) collective-permute-start(bf16[4,8,64,128]{3,2,1,0:T(8,128)(2,1)S(1)} %collective-permute-done.10.refs_2_), channel_id=1, source_target_pairs={{0,224},{32,0},{64,32},{96,64},{128,96},{160,128},{192,160},{224,1... | collective-permute-start | bytes 1572872 | tf_op jit(solution)/shard_map/ppermute | solution.py:24
  73.4 29.0 %collective-permute-start.13 = (bf16[4,8,64,128]{3,2,1,0:T(8,128)(2,1)S(1)}, bf16[4,8,64,128]{3,2,1,0:T(8,128)(2,1)S(1)}, u32[]{:S(2)}, u32[]{:S(2)}) collective-permute-start(bf16[4,8,64,128]{3,2,1,0:T(8,128)(2,1)S(1)} %collective-permute-done.11.refs_6_), channel_id=1, source_target_pairs={{0,32},{32,64},{64,96},{96,128},{128,160},{160,192},{192,224},{224... | collective-permute-start | bytes 1572872 | tf_op jit(solution)/shard_map/ppermute | solution.py:24
  86.2 17.3 %collective-permute-start.7 = (bf16[192,2048]{1,0:T(8,128)(2,1)S(1)}, bf16[192,2048]{1,0:T(8,128)(2,1)S(1)}, u32[]{:S(2)}, u32[]{:S(2)}) collective-permute-start(bf16[192,2048]{1,0:T(8,128)(2,1)S(1)} %all_gather.21.mine_ref), channel_id=1, source_target_pairs={{0,1},{1,0},{2,3},{3,2},{4,5},{5,4},{6,7},{7,6},{8,9},{9,8},{10,11... | collective-permute-start | bytes 2359304 | tf_op jit(solution)/shard_map/ppermute | solution.py:24
  96.2 23.2 %collective-permute-start.17 = (bf16[8,5,64,128]{3,2,1,0:T(8,128)(2,1)S(1)}, bf16[8,5,64,128]{3,2,1,0:T(8,128)(2,1)S(1)}, u32[]{:S(2)}, u32[]{:S(2)}) collective-permute-start(bf16[8,5,64,128]{3,2,1,0:T(8,128)(2,1)S(1)} %slice.24), channel_id=1, source_target_pairs={{0,24},{8,0},{16,8},{24,16},{1,25},{9,1},{17,9},{25,17},{2,26},{10... | collective-permute-start | bytes 1966088 | tf_op jit(solution)/shard_map/ppermute | solution.py:24
  102.3 16.6 %collective-permute-start.18 = (bf16[8,4,64,128]{3,2,1,0:T(8,128)(2,1)S(1)}, bf16[8,4,64,128]{3,2,1,0:T(8,128)(2,1)S(1)}, u32[]{:S(2)}, u32[]{:S(2)}) collective-permute-start(bf16[8,4,64,128]{3,2,1,0:T(8,128)(2,1)S(1)} %slice.25), channel_id=1, source_target_pairs={{0,8},{8,16},{16,24},{24,0},{1,9},{9,17},{17,25},{25,1},{2,10},{10... | collective-permute-start | bytes 1572872 | tf_op jit(solution)/shard_map/ppermute | solution.py:24
  102.4 16.9 %collective-permute-start.14 = (bf16[4,8,64,128]{3,2,1,0:T(8,128)(2,1)S(1)}, bf16[4,8,64,128]{3,2,1,0:T(8,128)(2,1)S(1)}, u32[]{:S(2)}, u32[]{:S(2)}) collective-permute-start(bf16[4,8,64,128]{3,2,1,0:T(8,128)(2,1)S(1)} %collective-permute-done.12.refs_3_), channel_id=1, source_target_pairs={{0,224},{32,0},{64,32},{96,64},{128,96},{160,128},{192,160},{224,1... | collective-permute-start | bytes 1572872 | tf_op jit(solution)/shard_map/ppermute | solution.py:24
  127.9 15.4 %all-to-all-start = ((bf16[4,48,2048]{2,1,0:T(8,128)(2,1)}), bf16[4,48,2048]{2,1,0:T(8,128)(2,1)S(1)}, u32[]{:S(2)}, u32[]{:S(2)}) async-start(bf16[4,48,2048]{2,1,0:T(8,128)(2,1)} %shard_map.166), calls=%async_computation | async-start | bytes 1572864 | tf_op jit(solution)/shard_map/all_to_all | solution.py:113
  155.5 6.1 %collective-permute-start.20 = (bf16[192,2048]{1,0:T(8,128)(2,1)S(1)}, bf16[192,2048]{1,0:T(8,128)(2,1)S(1)}, u32[]{:S(2)}, u32[]{:S(2)}) collective-permute-start(bf16[192,2048]{1,0:T(8,128)(2,1)S(1)} %all_gather.25.mine_ref), channel_id=1, source_target_pairs={{0,1},{1,0},{2,3},{3,2},{4,5},{5,4},{6,7},{7,6},{8,9},{9,8},{10,11... | collective-permute-start | bytes 2359304 | tf_op jit(solution)/shard_map/ppermute | solution.py:24
  196.7 6.0 %collective-permute-start.22 = (bf16[192,2048]{1,0:T(8,128)(2,1)S(1)}, bf16[192,2048]{1,0:T(8,128)(2,1)S(1)}, u32[]{:S(2)}, u32[]{:S(2)}) collective-permute-start(bf16[192,2048]{1,0:T(8,128)(2,1)S(1)} %all_gather.26.mine_ref), channel_id=1, source_target_pairs={{0,1},{1,0},{2,3},{3,2},{4,5},{5,4},{6,7},{7,6},{8,9},{9,8},{10,11... | collective-permute-start | bytes 2359304 | tf_op jit(solution)/shard_map/ppermute | solution.py:24
  212.6 11.6 %collective-permute-start.24 = (bf16[48,2048]{1,0:T(8,128)(2,1)S(1)}, bf16[48,2048]{1,0:T(8,128)(2,1)S(1)}, u32[]{:S(2)}, u32[]{:S(2)}) collective-permute-start(bf16[48,2048]{1,0:T(8,128)(2,1)S(1)} %get-tuple-element.74), channel_id=1, source_target_pairs={{0,2},{2,4},{4,6},{6,0},{1,3},{3,5},{5,7},{7,1},{8,10},{10,12},{12... | collective-permute-start | bytes 589832 | tf_op jit(solution)/shard_map/ppermute | solution.py:24
  212.7 11.5 %collective-permute-start.25 = (bf16[48,2048]{1,0:T(8,128)(2,1)S(1)}, bf16[48,2048]{1,0:T(8,128)(2,1)S(1)}, u32[]{:S(2)}, u32[]{:S(2)}) collective-permute-start(bf16[48,2048]{1,0:T(8,128)(2,1)S(1)} %get-tuple-element.75), channel_id=1, source_target_pairs={{0,4},{2,6},{4,0},{6,2},{1,5},{3,7},{5,1},{7,3},{8,12},{10,14},{12... | collective-permute-start | bytes 589832 | tf_op jit(solution)/shard_map/ppermute | solution.py:24
  214.1 10.5 %collective-permute-start.26 = (bf16[48,2048]{1,0:T(8,128)(2,1)S(1)}, bf16[48,2048]{1,0:T(8,128)(2,1)S(1)}, u32[]{:S(2)}, u32[]{:S(2)}) collective-permute-start(bf16[48,2048]{1,0:T(8,128)(2,1)S(1)} %get-tuple-element.76), channel_id=1, source_target_pairs={{0,6},{2,0},{4,2},{6,4},{1,7},{3,1},{5,3},{7,5},{8,14},{10,8},{12,... | collective-permute-start | bytes 589832 | tf_op jit(solution)/shard_map/ppermute | solution.py:24
  (16 other events, 161.0 us)
Sparse Core Ops, SparseCore 0:
  9.9 85.4 all-gather.3
  98.0 98.2 all-gather.5

commit v2 on v1

--- a/solution.py
+++ b/solution.py
@@ -15,7 +15,6 @@
 SHARD = 64
 HALF = 64
 WIDE = 256
-FFN_LOOPED = (False, False)
 PARAMS = pltpu.CompilerParams(vmem_limit_bytes=24 << 20)
 
 
@@ -197,6 +196,24 @@
     return full.reshape(-1, *packed.shape)
 
 
+def fetch_kernel(in_ref, out_ref, sem):
+    copy = pltpu.make_async_copy(in_ref, out_ref, sem)
+    copy.start()
+    copy.wait()
+
+
+def fetched(value):
+    return pl.pallas_call(
+        fetch_kernel,
+        in_specs=[pl.BlockSpec(memory_space=pl.ANY)],
+        out_specs=vmem_specs(1)[0],
+        out_shape=pltpu.VMEM(value.shape, value.dtype),
+        scratch_shapes=[pltpu.SemaphoreType.DMA],
+        compiler_params=PARAMS,
+        name="copy_in",
+    )(in_hbm(value))
+
+
 def full_tiles(which, count):
     return [((which, k * LANES, LANES),) for k in range(count)]
 
@@ -264,7 +281,7 @@
     return pl.ds(n * size if isinstance(n, int) else pl.multiple_of(n * size, size), size)
 
 
-def ffn_steps(looped, tile, down, mine_ref, other_ref, out_mine_ref, out_other_ref, hidden_ref, rows_ref):
+def ffn_steps(tile, down, mine_ref, other_ref, out_mine_ref, out_other_ref, hidden_ref, rows_ref):
     half = mine_ref.shape[0]
     rows_ref[:half] = mine_ref[...]
     rows_ref[half:] = other_ref[...]
@@ -275,7 +292,7 @@
         hidden = pair[:, :LANES] * jax.nn.sigmoid(pair[:, :LANES]) * pair[:, LANES:]
         hidden_ref[:, lanes(n, LANES)] = hidden.astype(jnp.bfloat16)
 
-    steps(5, hidden_step, looped[0])
+    steps(5, hidden_step, False)
     pair = jnp.dot(rows_ref[...], tile(10), preferred_element_type=jnp.float32)
     hidden = pair * jax.nn.sigmoid(pair) * pltpu.roll(pair, HALF, 1)
     lane = lax.broadcasted_iota(jnp.int32, hidden.shape, 1)
@@ -287,7 +304,7 @@
         out_mine_ref[:, lanes(n, WIDE)] = terms[:half]
         out_other_ref[:, lanes(n, WIDE)] = terms[half:]
 
-    steps(8, down_step, looped[1])
+    steps(8, down_step, False)
 
 
 def first_ffn_kernel(mine_ref, other_ref, *refs):
@@ -306,24 +323,79 @@
         block, which = (block_a, 6 + k) if k < 2 else (block_b, k - 2)
         return jnp.concatenate([block(which, n) for n in range(8)], axis=0)
 
-    ffn_steps((False, False), tile, block_a, mine_ref, other_ref, *refs[13:])
-
-
-def ffn_kernel(mine_ref, other_ref, packed_ref, *refs):
-    def down(k, n):
-        return packed_ref[pl.ds(n * 4, 4), k].reshape(-1, LANES)
-
-    ffn_steps(FFN_LOOPED, lambda k: packed_ref[:, 6 + k].reshape(-1, LANES), down, mine_ref, other_ref, *refs)
-
-
-def ffn_terms(rows, kernel, weights):
-    half, width = rows[0].shape
-    scratch = [
+    ffn_steps(tile, block_a, mine_ref, other_ref, *refs[13:])
+
+
+def ffn_kernel(
+    mine_ref, other_ref, packed_ref, out_mine_ref, out_other_ref, hidden_ref, rows_ref, store_ref, sum_ref, sems
+):
+    half = mine_ref.shape[0]
+    tiles = store_ref.shape[1]
+
+    def copy(n):
+        own = pl.ds(n * 4, 4)
+        return pltpu.make_async_copy(packed_ref.at[own], store_ref.at[own], sems.at[n])
+
+    for n in range(8):
+        copy(n).start()
+    rows_ref[:half] = mine_ref[...]
+    rows_ref[half:] = other_ref[...]
+    sum_ref[...] = jnp.zeros_like(sum_ref)
+
+    def chunk(n, carry):
+        copy(n).wait()
+        own = pl.ds(n * 4, 4)
+        both = jnp.concatenate([store_ref[own, k].reshape(-1, LANES) for k in range(6, tiles)], axis=1)
+        part = rows_ref[:, lanes(n, WIDE)]
+        sum_ref[...] += jnp.dot(part, both, preferred_element_type=jnp.float32)
+        return carry
+
+    lax.fori_loop(0, 8, chunk, 0)
+    for n in range(5):
+        gate = sum_ref[:, lanes(n, LANES)]
+        hidden = gate * jax.nn.sigmoid(gate) * sum_ref[:, lanes(5 + n, LANES)]
+        hidden_ref[:, lanes(n, LANES)] = hidden.astype(jnp.bfloat16)
+    pair = sum_ref[:, lanes(10, LANES)]
+    hidden = pair * jax.nn.sigmoid(pair) * pltpu.roll(pair, HALF, 1)
+    lane = lax.broadcasted_iota(jnp.int32, hidden.shape, 1)
+    hidden_ref[:, lanes(5, LANES)] = jnp.where(lane < HALF, hidden, 0.0).astype(jnp.bfloat16)
+    for n in range(8):
+        own = pl.ds(n * 4, 4)
+        both = jnp.concatenate([store_ref[own, k].reshape(-1, LANES) for k in range(6)], axis=1)
+        terms = nt_dot(hidden_ref[...], both).astype(jnp.bfloat16)
+        out_mine_ref[:, lanes(n, WIDE)] = terms[:half]
+        out_other_ref[:, lanes(n, WIDE)] = terms[half:]
+
+
+def ffn_scratch(half, width):
+    return [
         pltpu.VMEM((2 * half, 6 * LANES), jnp.bfloat16),
         pltpu.VMEM((2 * half, width), jnp.bfloat16),
     ]
-    outs = [pltpu.VMEM((half, width), jnp.bfloat16)] * 2
-    return vmem_call(kernel, outs, scratch)(*rows, *weights)
+
+
+def first_ffn_terms(rows, weights):
+    outs = [pltpu.VMEM(rows[0].shape, jnp.bfloat16)] * 2
+    call = vmem_call(first_ffn_kernel, outs, ffn_scratch(*rows[0].shape))
+    return call(*rows, *weights)
+
+
+def ffn_terms(rows, packed):
+    half, width = rows[0].shape
+    return pl.pallas_call(
+        ffn_kernel,
+        in_specs=vmem_specs(2) + [pl.BlockSpec(memory_space=pl.ANY)],
+        out_specs=vmem_specs(2),
+        out_shape=[pltpu.VMEM((half, width), jnp.bfloat16)] * 2,
+        scratch_shapes=[
+            *ffn_scratch(half, width),
+            pltpu.VMEM(packed.shape, jnp.bfloat16),
+            pltpu.VMEM((2 * half, (packed.shape[1] - 6) * LANES), jnp.float32),
+            pltpu.SemaphoreType.DMA((8,)),
+        ],
+        compiler_params=PARAMS,
+        name="ffn",
+    )(*in_vmem(*rows), in_hbm(packed))
 
 
 def shifted(values, by, fill):
@@ -476,17 +548,16 @@
     normed = turned_norm(tokens, ffn1_gain)
     normed = after(normed, block)
     rows = gather_rows(normed)
-    sums = sent_sums(ffn_terms(rows, first_ffn_kernel, weights))
+    sums = sent_sums(first_ffn_terms(rows, weights))
     first, normed = combined(tokens, sums, True, "zy", mix_gain)
-    (packed_mixing,) = in_vmem(packed_mixing)
-    normed, packed_mixing = lax.optimization_barrier((normed, packed_mixing))
+    packed_mixing = fetched(packed_mixing)
     rows = gather_rows(normed)
     sums = sent_sums(
         mixer_terms(rows, packed_mixing, conv_weight, gate_a_weight, gate_x_weight, decay_param),
     )
     second, normed = combined(first, sums, False, "", ffn2_gain)
     rows = gather_rows(normed)
-    sums = last_sums(ffn_terms(rows, ffn_kernel, [packed]))
+    sums = last_sums(ffn_terms(rows, packed))
     return combined(second, sums, True)[0]
 
 

time: 233 us -> 229 us (0.983)
  local copies, waits for them, and re-layouts: 5.41 us -> 0.14 us
  Pallas kernels: 17.9 us -> 22.5 us
    pallas_call x0 -> x2, Pallas kernels: none -> 8.38 us  [the longest x1 6.58 us: ffn_terms(): pl.pallas_call(ffn_kernel, in_specs=vmem_specs(2) + [pl.BlockSpec(memory_...]
    unnamed x20 -> x16, local copies, waits for them, and re-layouts: 5.31 us -> 0.04 us
    pallas_call x11 -> x10, Pallas kernels: 15.9 us -> 12 us  [call(): pl.pallas_call(kernel, in_specs=vmem_specs(len(args)), out_specs=jax.tree...]
  transfers between devices with their start and end apart: 30 -> 30, of which waited for: 17 -> 16; matrix products, arithmetic and copies ran while one was open for 0% -> 0% of each run, Pallas kernels for 5% -> 6%
where the time goes in v2:
time: 229 us
  waiting for transfers between devices  76.3 us (33%)
  blocking collectives  60.8 us (27%)
  starting transfers between devices  55 us (24%)
  Pallas kernels  22.5 us (10%)
  between operations  13.7 us (6%)
    ppermute x27, waiting for transfers between devices, moved(): lax.ppermute(value, axis, [(i, (i - by) % count) for i in range(count)])  63.7 us
    ppermute x27, starting transfers between devices, moved(): lax.ppermute(value, axis, [(i, (i - by) % count) for i in range(count)])  51.5 us
    all_gather x3, blocking collectives, gather_rows(): mine = lax.all_gather(own, 'x', axis=0, tiled=True)  34.9 us
    all_to_all x1, blocking collectives, sent_sums(): return [lax.all_to_all(sums, 'x', split_axis=0, concat_axis=0, tiled=True)]  14.4 us
    pallas_call x10, Pallas kernels, call(): pl.pallas_call(kernel, in_specs=vmem_specs(len(args)), out_specs=jax.tree...  12 us
    all_to_all x1, waiting for transfers between devices, sent_sums(): return [lax.all_to_all(sums, 'x', split_axis=0, concat_axis=0, tiled=True)]  11.9 us
    all_gather x1, blocking collectives, body(): own = lax.all_gather(own, 'y', axis=0)  11.4 us
    pallas_call x1, Pallas kernels, ffn_terms(): pl.pallas_call(ffn_kernel, in_specs=vmem_specs(2) + [pl.BlockSpec(memory_...  6.58 us
  transfers between devices with their start and end apart: 30, of which 16 were waited for; matrix products, arithmetic and copies ran while one was open for 0% of the time, Pallas kernels for 6%

profile of v2, /device:TPU:1, one launch (start us, length us, event | category | flops | bytes accessed | tf_op | source)
XLA Modules:
  0.0 228.6 jit_solution(10548665496968657451)
XLA Ops:
  9.4 6.5 %collective-permute-start = (bf16[9,64,128]{2,1,0:T(8,128)(2,1)S(1)}, bf16[9,64,128]{2,1,0:T(8,128)(2,1)S(1)}, u32[]{:S(2)}, u32[]{:S(2)}) collective-permute-start(bf16[9,64,128]{2,1,0:T(8,128)(2,1)S(1)} %get-tuple-element.39.refs_0_), channel_id=1, source_target_pairs={{0,224},{32,0},{64,32},{96,64},{128,96},{160,128},{192,160},{224,1... | collective-permute-start | bytes 442376 | tf_op jit(solution)/shard_map/ppermute | solution.py:23
  18.4 3.1 %collective-permute-done.1.refs_7_ = bf16[9,64,128]{2,1,0:T(8,128)(2,1)S(1)} collective-permute-done((bf16[9,64,128]{2,1,0:T(8,128)(2,1)S(1)}, bf16[9,64,128]{2,1,0:T(8,128)(2,1)S(1)}, u32[]{:S(2)}, u32[]{:S(2)}) %collective-permute-start.1) | collective-permute-done | bytes 147488 | tf_op jit(solution)/shard_map/ppermute | solution.py:23
  28.5 11.4 %all-gather = bf16[32,64,128]{2,1,0:T(8,128)(2,1)S(1)} all-gather(bf16[8,64,128]{2,1,0:T(8,128)(2,1)S(1)} %get-tuple-element.47), channel_id=2, replica_groups=mesh['z'=8,'y'=4,'x'=4,'c'=2] {'y'}, dimensions={0}, use_global_device_ids=true | all-gather | bytes 655360 | tf_op jit(solution)/shard_map/all_gather | solution.py:544
  41.5 2.6 %collective-permute-start.6 = (bf16[9,64,128]{2,1,0:T(8,128)(2,1)S(1)}, bf16[9,64,128]{2,1,0:T(8,128)(2,1)S(1)}, u32[]{:S(2)}, u32[]{:S(2)}) collective-permute-start(bf16[9,64,128]{2,1,0:T(8,128)(2,1)S(1)} %collective-permute-done.4.refs_3_), channel_id=1, source_target_pairs={{0,224},{32,0},{64,32},{96,64},{128,96},{160,128},{192,160},{224,1... | collective-permute-start | bytes 442376 | tf_op jit(solution)/shard_map/ppermute | solution.py:23
  44.1 8.9 %collective-permute-done.6.refs_4_ = bf16[9,64,128]{2,1,0:T(8,128)(2,1)S(1)} collective-permute-done((bf16[9,64,128]{2,1,0:T(8,128)(2,1)S(1)}, bf16[9,64,128]{2,1,0:T(8,128)(2,1)S(1)}, u32[]{:S(2)}, u32[]{:S(2)}) %collective-permute-start.6) | collective-permute-done | bytes 147488 | tf_op jit(solution)/shard_map/ppermute | solution.py:23
  53.1 3.4 %collective-permute-start.15 = (bf16[8,9,64,128]{3,2,1,0:T(8,128)(2,1)S(1)}, bf16[8,9,64,128]{3,2,1,0:T(8,128)(2,1)S(1)}, u32[]{:S(2)}, u32[]{:S(2)}) collective-permute-start(bf16[8,9,64,128]{3,2,1,0:T(8,128)(2,1)S(1)} %shard_map.164.refs_8_), channel_id=1, source_target_pairs={{0,24},{8,0},{16,8},{24,16},{1,25},{9,1},{17,9},{25,17},{2,26},{10... | collective-permute-start | bytes 3538952 | tf_op jit(solution)/shard_map/ppermute | solution.py:23
  56.4 3.1 %collective-permute-start.10 = (bf16[4,8,64,128]{3,2,1,0:T(8,128)(2,1)S(1)}, bf16[4,8,64,128]{3,2,1,0:T(8,128)(2,1)S(1)}, u32[]{:S(2)}, u32[]{:S(2)}) collective-permute-start(bf16[4,8,64,128]{3,2,1,0:T(8,128)(2,1)S(1)} %collective-permute-done.8.refs_1_), channel_id=1, source_target_pairs={{0,224},{32,0},{64,32},{96,64},{128,96},{160,128},{192,160},{224,1... | collective-permute-start | bytes 1572872 | tf_op jit(solution)/shard_map/ppermute | solution.py:23
  60.0 9.5 %collective-permute-done.10.refs_2_ = bf16[4,8,64,128]{3,2,1,0:T(8,128)(2,1)S(1)} collective-permute-done((bf16[4,8,64,128]{3,2,1,0:T(8,128)(2,1)S(1)}, bf16[4,8,64,128]{3,2,1,0:T(8,128)(2,1)S(1)}, u32[]{:S(2)}, u32[]{:S(2)}) %collective-permute-start.10) | collective-permute-done | bytes 524320 | tf_op jit(solution)/shard_map/ppermute | solution.py:23
  69.4 3.3 %collective-permute-done.11.refs_6_ = bf16[4,8,64,128]{3,2,1,0:T(8,128)(2,1)S(1)} collective-permute-done((bf16[4,8,64,128]{3,2,1,0:T(8,128)(2,1)S(1)}, bf16[4,8,64,128]{3,2,1,0:T(8,128)(2,1)S(1)}, u32[]{:S(2)}, u32[]{:S(2)}) %collective-permute-start.11) | collective-permute-done | bytes 524320 | tf_op jit(solution)/shard_map/ppermute | solution.py:23
  74.1 11.9 %all_gather.21.mine_ref = bf16[192,2048]{1,0:T(8,128)(2,1)S(1)} all-gather(bf16[48,2048]{1,0:T(8,128)(2,1)S(1)} %shard_map.163), channel_id=1, replica_groups=mesh['z'=8,'y'=4,'x'=4,'c'=2] {'x'}, dimensions={0}, use_global_device_ids=true | all-gather | bytes 983040 | tf_op jit(solution)/shard_map/all_gather | solution.py:93
  86.0 10.7 %collective-permute-start.7 = (bf16[192,2048]{1,0:T(8,128)(2,1)S(1)}, bf16[192,2048]{1,0:T(8,128)(2,1)S(1)}, u32[]{:S(2)}, u32[]{:S(2)}) collective-permute-start(bf16[192,2048]{1,0:T(8,128)(2,1)S(1)} %all_gather.21.mine_ref), channel_id=1, source_target_pairs={{0,1},{1,0},{2,3},{3,2},{4,5},{5,4},{6,7},{7,6},{8,9},{9,8},{10,11... | collective-permute-start | bytes 2359304 | tf_op jit(solution)/shard_map/ppermute | solution.py:23
  96.7 5.3 %collective-permute-start.17 = (bf16[8,5,64,128]{3,2,1,0:T(8,128)(2,1)S(1)}, bf16[8,5,64,128]{3,2,1,0:T(8,128)(2,1)S(1)}, u32[]{:S(2)}, u32[]{:S(2)}) collective-permute-start(bf16[8,5,64,128]{3,2,1,0:T(8,128)(2,1)S(1)} %slice.24), channel_id=1, source_target_pairs={{0,24},{8,0},{16,8},{24,16},{1,25},{9,1},{17,9},{25,17},{2,26},{10... | collective-permute-start | bytes 1966088 | tf_op jit(solution)/shard_map/ppermute | solution.py:23
  103.2 15.3 %collective-permute-done.18.refs_11_ = bf16[8,4,64,128]{3,2,1,0:T(8,128)(2,1)S(1)} collective-permute-done((bf16[8,4,64,128]{3,2,1,0:T(8,128)(2,1)S(1)}, bf16[8,4,64,128]{3,2,1,0:T(8,128)(2,1)S(1)}, u32[]{:S(2)}, u32[]{:S(2)}) %collective-permute-start.18) | collective-permute-done | bytes 524320 | tf_op jit(solution)/shard_map/ppermute | solution.py:23
  119.1 3.8 %shard_map.165 = (bf16[192,2048]{1,0:T(8,128)(2,1)S(1)}, bf16[192,2048]{1,0:T(8,128)(2,1)S(1)}) custom-call(bf16[192,2048]{1,0:T(8,128)(2,1)S(1)} %all_gather.21.mine_ref, bf16[192,2048]{1,0:T(8,128)(2,1)S(1)} %collective-permute-done.7.other_ref, bf16[4,8,64,128]{3,2,1,0:T(8,128)(2,1)S(1)} %bitcast.34, ...), custom_call_target="tpu_custom_call" | custom-call | tf_op jit(solution)/shard_map/pallas_call | solution.py:36
  127.4 3.5 %all-to-all-start = ((bf16[4,48,2048]{2,1,0:T(8,128)(2,1)}), bf16[4,48,2048]{2,1,0:T(8,128)(2,1)S(1)}, u32[]{:S(2)}, u32[]{:S(2)}) async-start(bf16[4,48,2048]{2,1,0:T(8,128)(2,1)} %shard_map.166), calls=%async_computation | async-start | bytes 1572864 | tf_op jit(solution)/shard_map/all_to_all | solution.py:112
  131.0 11.9 %all-to-all-done.refs_1_ = bf16[4,48,2048]{2,1,0:T(8,128)(2,1)S(1)} async-done(((bf16[4,48,2048]{2,1,0:T(8,128)(2,1)}), bf16[4,48,2048]{2,1,0:T(8,128)(2,1)S(1)}, u32[]{:S(2)}, u32[]{:S(2)}) %all-to-all-start) | async-done | bytes 786464 | tf_op jit(solution)/shard_map/all_to_all | solution.py:112
  143.4 11.4 %all_gather.24.mine_ref = bf16[192,2048]{1,0:T(8,128)(2,1)S(1)} all-gather(bf16[48,2048]{1,0:T(8,128)(2,1)S(1)} %get-tuple-element.60), channel_id=1, replica_groups=mesh['z'=8,'y'=4,'x'=4,'c'=2] {'x'}, dimensions={0}, use_global_device_ids=true | all-gather | bytes 983040 | tf_op jit(solution)/shard_map/all_gather | solution.py:93
  154.9 4.0 %collective-permute-start.20 = (bf16[192,2048]{1,0:T(8,128)(2,1)S(1)}, bf16[192,2048]{1,0:T(8,128)(2,1)S(1)}, u32[]{:S(2)}, u32[]{:S(2)}) collective-permute-start(bf16[192,2048]{1,0:T(8,128)(2,1)S(1)} %all_gather.24.mine_ref), channel_id=1, source_target_pairs={{0,1},{1,0},{2,3},{3,2},{4,5},{5,4},{6,7},{7,6},{8,9},{9,8},{10,11... | collective-permute-start | bytes 2359304 | tf_op jit(solution)/shard_map/ppermute | solution.py:23
  160.9 4.7 %shard_map.168 = (bf16[192,2048]{1,0:T(8,128)(2,1)S(1)}, bf16[192,2048]{1,0:T(8,128)(2,1)S(1)}) custom-call(bf16[192,2048]{1,0:T(8,128)(2,1)S(1)} %all_gather.24.mine_ref, bf16[192,2048]{1,0:T(8,128)(2,1)S(1)} %collective-permute-done.20.other_ref, bf16[32,5,64,128]{3,2,1,0:T(8,128)(2,1)S(1)} %copy_in.1.packed_ref, f32[4,256]{1,0:T(4,128)S(1)} %pad_convert_fusion.taps_ref, ...), custom_call_target="tpu_custom_call" | custom-call | tf_op jit(solution)/shard_map/pallas_call | solution.py:36
  168.2 14.4 %all_to_all.10.refs_1_ = bf16[4,48,2048]{2,1,0:T(8,128)(2,1)S(1)} all-to-all(bf16[4,48,2048]{2,1,0:T(8,128)(2,1)S(1)} %shard_map.169), channel_id=1, replica_groups=mesh['z'=8,'y'=4,'x'=4,'c'=2] {'x'}, dimensions={0} | all-to-all | bytes 1572864 | tf_op jit(solution)/shard_map/all_to_all | solution.py:112
  182.9 11.6 %all_gather.26.mine_ref = bf16[192,2048]{1,0:T(8,128)(2,1)S(1)} all-gather(bf16[48,2048]{1,0:T(8,128)(2,1)S(1)} %get-tuple-element.65), channel_id=1, replica_groups=mesh['z'=8,'y'=4,'x'=4,'c'=2] {'x'}, dimensions={0}, use_global_device_ids=true | all-gather | bytes 983040 | tf_op jit(solution)/shard_map/all_gather | solution.py:93
  194.6 3.4 %collective-permute-start.22 = (bf16[192,2048]{1,0:T(8,128)(2,1)S(1)}, bf16[192,2048]{1,0:T(8,128)(2,1)S(1)}, u32[]{:S(2)}, u32[]{:S(2)}) collective-permute-start(bf16[192,2048]{1,0:T(8,128)(2,1)S(1)} %all_gather.26.mine_ref), channel_id=1, source_target_pairs={{0,1},{1,0},{2,3},{3,2},{4,5},{5,4},{6,7},{7,6},{8,9},{9,8},{10,11... | collective-permute-start | bytes 2359304 | tf_op jit(solution)/shard_map/ppermute | solution.py:23
  199.9 6.6 %ffn.1 = (bf16[192,2048]{1,0:T(8,128)(2,1)S(1)}, bf16[192,2048]{1,0:T(8,128)(2,1)S(1)}) custom-call(bf16[192,2048]{1,0:T(8,128)(2,1)S(1)} %all_gather.26.mine_ref, bf16[192,2048]{1,0:T(8,128)(2,1)S(1)} %collective-permute-done.22.other_ref, bf16[32,17,64,128]{3,2,1,0:T(8,128)(2,1)} %bitcast.38), custom_call_target="tpu_custom_call" | custom-call | tf_op jit(solution)/shard_map/ffn/pallas_call | solution.py:385
  212.3 8.3 %collective-permute-done.24.refs_2_ = bf16[48,2048]{1,0:T(8,128)(2,1)S(1)} collective-permute-done((bf16[48,2048]{1,0:T(8,128)(2,1)S(1)}, bf16[48,2048]{1,0:T(8,128)(2,1)S(1)}, u32[]{:S(2)}, u32[]{:S(2)}) %collective-permute-start.24) | collective-permute-done | bytes 196640 | tf_op jit(solution)/shard_map/ppermute | solution.py:23
  (83 shorter events, 36.4 us)
Async XLA Ops:
  6.5 152.6 %all-gather.4.cloned.1.call-start = ((), (), s32[]{:S(2)}) async-start(), calls=%async_computation.2 | async-start | bytes 2703360 | tf_op jit(solution)/shard_map/all_gather | solution.py:195
  8.7 191.2 %all-gather.6.cloned.1.call-start = ((), (), s32[]{:S(2)}) async-start(), calls=%async_computation.3 | async-start | bytes 9191424 | tf_op jit(solution)/shard_map/all_gather | solution.py:195
  9.4 9.0 %collective-permute-start = (bf16[9,64,128]{2,1,0:T(8,128)(2,1)S(1)}, bf16[9,64,128]{2,1,0:T(8,128)(2,1)S(1)}, u32[]{:S(2)}, u32[]{:S(2)}) collective-permute-start(bf16[9,64,128]{2,1,0:T(8,128)(2,1)S(1)} %get-tuple-element.39.refs_0_), channel_id=1, source_target_pairs={{0,224},{32,0},{64,32},{96,64},{128,96},{160,128},{192,160},{224,1... | collective-permute-start | bytes 442376 | tf_op jit(solution)/shard_map/ppermute | solution.py:23
  15.9 5.7 %collective-permute-start.1 = (bf16[9,64,128]{2,1,0:T(8,128)(2,1)S(1)}, bf16[9,64,128]{2,1,0:T(8,128)(2,1)S(1)}, u32[]{:S(2)}, u32[]{:S(2)}) collective-permute-start(bf16[9,64,128]{2,1,0:T(8,128)(2,1)S(1)} %get-tuple-element.39.refs_0_), channel_id=1, source_target_pairs={{0,32},{32,64},{64,96},{96,128},{128,160},{160,192},{192,224},{224... | collective-permute-start | bytes 442376 | tf_op jit(solution)/shard_map/ppermute | solution.py:23
  27.1 12.9 %collective-permute-start.4 = (bf16[9,64,128]{2,1,0:T(8,128)(2,1)S(1)}, bf16[9,64,128]{2,1,0:T(8,128)(2,1)S(1)}, u32[]{:S(2)}, u32[]{:S(2)}) collective-permute-start(bf16[9,64,128]{2,1,0:T(8,128)(2,1)S(1)} %collective-permute-done.2.refs_2_), channel_id=1, source_target_pairs={{0,224},{32,0},{64,32},{96,64},{128,96},{160,128},{192,160},{224,1... | collective-permute-start | bytes 442376 | tf_op jit(solution)/shard_map/ppermute | solution.py:23
  27.1 12.9 %collective-permute-start.5 = (bf16[9,64,128]{2,1,0:T(8,128)(2,1)S(1)}, bf16[9,64,128]{2,1,0:T(8,128)(2,1)S(1)}, u32[]{:S(2)}, u32[]{:S(2)}) collective-permute-start(bf16[9,64,128]{2,1,0:T(8,128)(2,1)S(1)} %collective-permute-done.3.refs_6_), channel_id=1, source_target_pairs={{0,32},{32,64},{64,96},{96,128},{128,160},{160,192},{192,224},{224... | collective-permute-start | bytes 442376 | tf_op jit(solution)/shard_map/ppermute | solution.py:23
  39.9 16.5 %collective-permute-start.8 = (bf16[4,8,64,128]{3,2,1,0:T(8,128)(2,1)S(1)}, bf16[4,8,64,128]{3,2,1,0:T(8,128)(2,1)S(1)}, u32[]{:S(2)}, u32[]{:S(2)}) collective-permute-start(bf16[4,8,64,128]{3,2,1,0:T(8,128)(2,1)S(1)} %bitcast.32), channel_id=1, source_target_pairs={{0,224},{32,0},{64,32},{96,64},{128,96},{160,128},{192,160},{224,1... | collective-permute-start | bytes 1572872 | tf_op jit(solution)/shard_map/ppermute | solution.py:23
  41.4 15.0 %collective-permute-start.9 = (bf16[4,8,64,128]{3,2,1,0:T(8,128)(2,1)S(1)}, bf16[4,8,64,128]{3,2,1,0:T(8,128)(2,1)S(1)}, u32[]{:S(2)}, u32[]{:S(2)}) collective-permute-start(bf16[4,8,64,128]{3,2,1,0:T(8,128)(2,1)S(1)} %bitcast.33), channel_id=1, source_target_pairs={{0,32},{32,64},{64,96},{96,128},{128,160},{160,192},{192,224},{224... | collective-permute-start | bytes 1572872 | tf_op jit(solution)/shard_map/ppermute | solution.py:23
  41.5 11.5 %collective-permute-start.6 = (bf16[9,64,128]{2,1,0:T(8,128)(2,1)S(1)}, bf16[9,64,128]{2,1,0:T(8,128)(2,1)S(1)}, u32[]{:S(2)}, u32[]{:S(2)}) collective-permute-start(bf16[9,64,128]{2,1,0:T(8,128)(2,1)S(1)} %collective-permute-done.4.refs_3_), channel_id=1, source_target_pairs={{0,224},{32,0},{64,32},{96,64},{128,96},{160,128},{192,160},{224,1... | collective-permute-start | bytes 442376 | tf_op jit(solution)/shard_map/ppermute | solution.py:23
  53.1 43.6 %collective-permute-start.15 = (bf16[8,9,64,128]{3,2,1,0:T(8,128)(2,1)S(1)}, bf16[8,9,64,128]{3,2,1,0:T(8,128)(2,1)S(1)}, u32[]{:S(2)}, u32[]{:S(2)}) collective-permute-start(bf16[8,9,64,128]{3,2,1,0:T(8,128)(2,1)S(1)} %shard_map.164.refs_8_), channel_id=1, source_target_pairs={{0,24},{8,0},{16,8},{24,16},{1,25},{9,1},{17,9},{25,17},{2,26},{10... | collective-permute-start | bytes 3538952 | tf_op jit(solution)/shard_map/ppermute | solution.py:23
  56.4 40.3 %collective-permute-start.16 = (bf16[8,9,64,128]{3,2,1,0:T(8,128)(2,1)S(1)}, bf16[8,9,64,128]{3,2,1,0:T(8,128)(2,1)S(1)}, u32[]{:S(2)}, u32[]{:S(2)}) collective-permute-start(bf16[8,9,64,128]{3,2,1,0:T(8,128)(2,1)S(1)} %shard_map.164.refs_8_), channel_id=1, source_target_pairs={{0,8},{8,16},{16,24},{24,0},{1,9},{9,17},{17,25},{25,1},{2,10},{10... | collective-permute-start | bytes 3538952 | tf_op jit(solution)/shard_map/ppermute | solution.py:23
  56.4 13.0 %collective-permute-start.10 = (bf16[4,8,64,128]{3,2,1,0:T(8,128)(2,1)S(1)}, bf16[4,8,64,128]{3,2,1,0:T(8,128)(2,1)S(1)}, u32[]{:S(2)}, u32[]{:S(2)}) collective-permute-start(bf16[4,8,64,128]{3,2,1,0:T(8,128)(2,1)S(1)} %collective-permute-done.8.refs_1_), channel_id=1, source_target_pairs={{0,224},{32,0},{64,32},{96,64},{128,96},{160,128},{192,160},{224,1... | collective-permute-start | bytes 1572872 | tf_op jit(solution)/shard_map/ppermute | solution.py:23
  59.5 13.1 %collective-permute-start.11 = (bf16[4,8,64,128]{3,2,1,0:T(8,128)(2,1)S(1)}, bf16[4,8,64,128]{3,2,1,0:T(8,128)(2,1)S(1)}, u32[]{:S(2)}, u32[]{:S(2)}) collective-permute-start(bf16[4,8,64,128]{3,2,1,0:T(8,128)(2,1)S(1)} %collective-permute-done.9.refs_7_), channel_id=1, source_target_pairs={{0,32},{32,64},{64,96},{96,128},{128,160},{160,192},{192,224},{224... | collective-permute-start | bytes 1572872 | tf_op jit(solution)/shard_map/ppermute | solution.py:23
  72.7 29.5 %collective-permute-start.12 = (bf16[4,8,64,128]{3,2,1,0:T(8,128)(2,1)S(1)}, bf16[4,8,64,128]{3,2,1,0:T(8,128)(2,1)S(1)}, u32[]{:S(2)}, u32[]{:S(2)}) collective-permute-start(bf16[4,8,64,128]{3,2,1,0:T(8,128)(2,1)S(1)} %collective-permute-done.10.refs_2_), channel_id=1, source_target_pairs={{0,224},{32,0},{64,32},{96,64},{128,96},{160,128},{192,160},{224,1... | collective-permute-start | bytes 1572872 | tf_op jit(solution)/shard_map/ppermute | solution.py:23
  73.0 29.2 %collective-permute-start.13 = (bf16[4,8,64,128]{3,2,1,0:T(8,128)(2,1)S(1)}, bf16[4,8,64,128]{3,2,1,0:T(8,128)(2,1)S(1)}, u32[]{:S(2)}, u32[]{:S(2)}) collective-permute-start(bf16[4,8,64,128]{3,2,1,0:T(8,128)(2,1)S(1)} %collective-permute-done.11.refs_6_), channel_id=1, source_target_pairs={{0,32},{32,64},{64,96},{96,128},{128,160},{160,192},{192,224},{224... | collective-permute-start | bytes 1572872 | tf_op jit(solution)/shard_map/ppermute | solution.py:23
  86.0 17.2 %collective-permute-start.7 = (bf16[192,2048]{1,0:T(8,128)(2,1)S(1)}, bf16[192,2048]{1,0:T(8,128)(2,1)S(1)}, u32[]{:S(2)}, u32[]{:S(2)}) collective-permute-start(bf16[192,2048]{1,0:T(8,128)(2,1)S(1)} %all_gather.21.mine_ref), channel_id=1, source_target_pairs={{0,1},{1,0},{2,3},{3,2},{4,5},{5,4},{6,7},{7,6},{8,9},{9,8},{10,11... | collective-permute-start | bytes 2359304 | tf_op jit(solution)/shard_map/ppermute | solution.py:23
  96.7 22.4 %collective-permute-start.17 = (bf16[8,5,64,128]{3,2,1,0:T(8,128)(2,1)S(1)}, bf16[8,5,64,128]{3,2,1,0:T(8,128)(2,1)S(1)}, u32[]{:S(2)}, u32[]{:S(2)}) collective-permute-start(bf16[8,5,64,128]{3,2,1,0:T(8,128)(2,1)S(1)} %slice.24), channel_id=1, source_target_pairs={{0,24},{8,0},{16,8},{24,16},{1,25},{9,1},{17,9},{25,17},{2,26},{10... | collective-permute-start | bytes 1966088 | tf_op jit(solution)/shard_map/ppermute | solution.py:23
  102.1 16.4 %collective-permute-start.18 = (bf16[8,4,64,128]{3,2,1,0:T(8,128)(2,1)S(1)}, bf16[8,4,64,128]{3,2,1,0:T(8,128)(2,1)S(1)}, u32[]{:S(2)}, u32[]{:S(2)}) collective-permute-start(bf16[8,4,64,128]{3,2,1,0:T(8,128)(2,1)S(1)} %slice.25), channel_id=1, source_target_pairs={{0,8},{8,16},{16,24},{24,0},{1,9},{9,17},{17,25},{25,1},{2,10},{10... | collective-permute-start | bytes 1572872 | tf_op jit(solution)/shard_map/ppermute | solution.py:23
  102.2 16.9 %collective-permute-start.14 = (bf16[4,8,64,128]{3,2,1,0:T(8,128)(2,1)S(1)}, bf16[4,8,64,128]{3,2,1,0:T(8,128)(2,1)S(1)}, u32[]{:S(2)}, u32[]{:S(2)}) collective-permute-start(bf16[4,8,64,128]{3,2,1,0:T(8,128)(2,1)S(1)} %collective-permute-done.12.refs_3_), channel_id=1, source_target_pairs={{0,224},{32,0},{64,32},{96,64},{128,96},{160,128},{192,160},{224,1... | collective-permute-start | bytes 1572872 | tf_op jit(solution)/shard_map/ppermute | solution.py:23
  127.4 15.5 %all-to-all-start = ((bf16[4,48,2048]{2,1,0:T(8,128)(2,1)}), bf16[4,48,2048]{2,1,0:T(8,128)(2,1)S(1)}, u32[]{:S(2)}, u32[]{:S(2)}) async-start(bf16[4,48,2048]{2,1,0:T(8,128)(2,1)} %shard_map.166), calls=%async_computation | async-start | bytes 1572864 | tf_op jit(solution)/shard_map/all_to_all | solution.py:112
  154.9 6.1 %collective-permute-start.20 = (bf16[192,2048]{1,0:T(8,128)(2,1)S(1)}, bf16[192,2048]{1,0:T(8,128)(2,1)S(1)}, u32[]{:S(2)}, u32[]{:S(2)}) collective-permute-start(bf16[192,2048]{1,0:T(8,128)(2,1)S(1)} %all_gather.24.mine_ref), channel_id=1, source_target_pairs={{0,1},{1,0},{2,3},{3,2},{4,5},{5,4},{6,7},{7,6},{8,9},{9,8},{10,11... | collective-permute-start | bytes 2359304 | tf_op jit(solution)/shard_map/ppermute | solution.py:23
  209.0 11.6 %collective-permute-start.24 = (bf16[48,2048]{1,0:T(8,128)(2,1)S(1)}, bf16[48,2048]{1,0:T(8,128)(2,1)S(1)}, u32[]{:S(2)}, u32[]{:S(2)}) collective-permute-start(bf16[48,2048]{1,0:T(8,128)(2,1)S(1)} %get-tuple-element.70), channel_id=1, source_target_pairs={{0,2},{2,4},{4,6},{6,0},{1,3},{3,5},{5,7},{7,1},{8,10},{10,12},{12... | collective-permute-start | bytes 589832 | tf_op jit(solution)/shard_map/ppermute | solution.py:23
  209.1 11.5 %collective-permute-start.25 = (bf16[48,2048]{1,0:T(8,128)(2,1)S(1)}, bf16[48,2048]{1,0:T(8,128)(2,1)S(1)}, u32[]{:S(2)}, u32[]{:S(2)}) collective-permute-start(bf16[48,2048]{1,0:T(8,128)(2,1)S(1)} %get-tuple-element.71), channel_id=1, source_target_pairs={{0,4},{2,6},{4,0},{6,2},{1,5},{3,7},{5,1},{7,3},{8,12},{10,14},{12... | collective-permute-start | bytes 589832 | tf_op jit(solution)/shard_map/ppermute | solution.py:23
  210.7 10.3 %collective-permute-start.26 = (bf16[48,2048]{1,0:T(8,128)(2,1)S(1)}, bf16[48,2048]{1,0:T(8,128)(2,1)S(1)}, u32[]{:S(2)}, u32[]{:S(2)}) collective-permute-start(bf16[48,2048]{1,0:T(8,128)(2,1)S(1)} %get-tuple-element.72), channel_id=1, source_target_pairs={{0,6},{2,0},{4,2},{6,4},{1,7},{3,1},{5,3},{7,5},{8,14},{10,8},{12,... | collective-permute-start | bytes 589832 | tf_op jit(solution)/shard_map/ppermute | solution.py:23
  (14 other events, 246.8 us)
Sparse Core Ops, SparseCore 0:
  9.9 85.3 all-gather.3
  97.8 98.5 all-gather.5

commit v3 on v2

--- a/solution.py
+++ b/solution.py
@@ -327,7 +327,17 @@
 
 
 def ffn_kernel(
-    mine_ref, other_ref, packed_ref, out_mine_ref, out_other_ref, hidden_ref, rows_ref, store_ref, sum_ref, sems
+    mine_ref,
+    other_ref,
+    mixing_ref,
+    packed_ref,
+    out_mine_ref,
+    out_other_ref,
+    hidden_ref,
+    rows_ref,
+    store_ref,
+    sum_ref,
+    sems,
 ):
     half = mine_ref.shape[0]
     tiles = store_ref.shape[1]
@@ -345,7 +355,7 @@
     def chunk(n, carry):
         copy(n).wait()
         own = pl.ds(n * 4, 4)
-        both = jnp.concatenate([store_ref[own, k].reshape(-1, LANES) for k in range(6, tiles)], axis=1)
+        both = jnp.concatenate([store_ref[own, k].reshape(-1, LANES) for k in range(5, tiles)], axis=1)
         part = rows_ref[:, lanes(n, WIDE)]
         sum_ref[...] += jnp.dot(part, both, preferred_element_type=jnp.float32)
         return carry
@@ -356,12 +366,13 @@
         hidden = gate * jax.nn.sigmoid(gate) * sum_ref[:, lanes(5 + n, LANES)]
         hidden_ref[:, lanes(n, LANES)] = hidden.astype(jnp.bfloat16)
     pair = sum_ref[:, lanes(10, LANES)]
-    hidden = pair * jax.nn.sigmoid(pair) * pltpu.roll(pair, HALF, 1)
+    hidden = pltpu.roll(pair * jax.nn.sigmoid(pair), HALF, 1) * pair
     lane = lax.broadcasted_iota(jnp.int32, hidden.shape, 1)
-    hidden_ref[:, lanes(5, LANES)] = jnp.where(lane < HALF, hidden, 0.0).astype(jnp.bfloat16)
+    hidden_ref[:, lanes(5, LANES)] = jnp.where(lane >= HALF, hidden, 0.0).astype(jnp.bfloat16)
     for n in range(8):
         own = pl.ds(n * 4, 4)
-        both = jnp.concatenate([store_ref[own, k].reshape(-1, LANES) for k in range(6)], axis=1)
+        down = [store_ref[own, k] for k in range(5)] + [mixing_ref[own, 4]]
+        both = jnp.concatenate([tile.reshape(-1, LANES) for tile in down], axis=1)
         terms = nt_dot(hidden_ref[...], both).astype(jnp.bfloat16)
         out_mine_ref[:, lanes(n, WIDE)] = terms[:half]
         out_other_ref[:, lanes(n, WIDE)] = terms[half:]
@@ -380,22 +391,22 @@
     return call(*rows, *weights)
 
 
-def ffn_terms(rows, packed):
+def ffn_terms(rows, mixing, packed):
     half, width = rows[0].shape
     return pl.pallas_call(
         ffn_kernel,
-        in_specs=vmem_specs(2) + [pl.BlockSpec(memory_space=pl.ANY)],
+        in_specs=vmem_specs(3) + [pl.BlockSpec(memory_space=pl.ANY)],
         out_specs=vmem_specs(2),
         out_shape=[pltpu.VMEM((half, width), jnp.bfloat16)] * 2,
         scratch_shapes=[
             *ffn_scratch(half, width),
             pltpu.VMEM(packed.shape, jnp.bfloat16),
-            pltpu.VMEM((2 * half, (packed.shape[1] - 6) * LANES), jnp.float32),
+            pltpu.VMEM((2 * half, (packed.shape[1] - 5) * LANES), jnp.float32),
             pltpu.SemaphoreType.DMA((8,)),
         ],
         compiler_params=PARAMS,
         name="ffn",
-    )(*in_vmem(*rows), in_hbm(packed))
+    )(*in_vmem(*rows, mixing), in_hbm(packed))
 
 
 def shifted(values, by, fill):
@@ -420,7 +431,7 @@
 
 
 def mixer_kernel(
-    mine_ref, other_ref, packed_ref, taps_ref, a_ref, b_ref, rate_ref, out_mine_ref, out_other_ref, order_ref
+    mine_ref, other_ref, packed_ref, taps_ref, a_ref, b_ref, rate_ref, out_mine_ref, out_other_ref, order_ref, group_ref
 ):
     half = mine_ref.shape[0]
     chips = lax.axis_size("x")
@@ -441,18 +452,16 @@
             place = pl.multiple_of((chip * 2 + which) * block, block)
             places.append(place)
             order_ref[pl.ds(place, block), :] = part[chip * block : (chip + 1) * block]
-    z = order_ref[:, : 2 * LANES]
     ends = order_ref[:, 2 * LANES :]
     lane = lax.broadcasted_iota(jnp.int32, ends.shape, 1)
-    groups = (
-        (z[:, :LANES], z[:, LANES:]),
-        (jnp.where(lane < HALF, ends, 0.0), pltpu.roll(ends, HALF, 1)),
-    )
-    mixed = []
-    for g, (lru_x, lru_gate) in enumerate(groups):
-        lru_x = lru_x.astype(jnp.bfloat16).astype(jnp.float32)
-        lru_gate = lru_gate.astype(jnp.bfloat16).astype(jnp.float32)
-        own = slice(g * LANES, (g + 1) * LANES)
+    group_ref[0] = order_ref[:, : 2 * LANES]
+    group_ref[1, :, :LANES] = jnp.where(lane < HALF, ends, 0.0)
+    group_ref[1, :, LANES:] = pltpu.roll(ends, HALF, 1)
+
+    def group(g, carry):
+        lru_x = group_ref[g, :, :LANES].astype(jnp.bfloat16).astype(jnp.float32)
+        lru_gate = group_ref[g, :, LANES:].astype(jnp.bfloat16).astype(jnp.float32)
+        own = lanes(g, LANES)
         taps = taps_ref[:, own]
         conv = taps[0:1] * lru_x
         for k in range(1, 4):
@@ -463,9 +472,10 @@
         log_keep = recall * rate_ref[:, own]
         drive = jnp.sqrt(minus_expm1(2.0 * log_keep)) * admit * low.astype(jnp.float32)
         state = scanned(jnp.exp(log_keep), drive)
-        mixed.append(state * jax.nn.gelu(lru_gate))
-    for g in range(2):
-        order_ref[:, g * LANES : (g + 1) * LANES] = mixed[g]
+        order_ref[:, own] = state * jax.nn.gelu(lru_gate)
+        return carry
+
+    lax.fori_loop(0, 2, group, 0)
     mixed = jnp.concatenate([order_ref[pl.ds(p, block), : 2 * LANES] for p in places], axis=0)
     mixed = mixed.astype(jnp.bfloat16)
     full = mixed[:, :LANES]
@@ -497,7 +507,10 @@
     taps = jnp.pad(conv_weight.astype(jnp.float32), pad)
     rate = jnp.pad(-8.0 * jax.nn.softplus(-decay_param)[None], pad)
     outs = [pltpu.VMEM((half, width), jnp.bfloat16)] * 2
-    scratch = [pltpu.VMEM((2 * half, 3 * LANES), jnp.float32)]
+    scratch = [
+        pltpu.VMEM((2 * half, 3 * LANES), jnp.float32),
+        pltpu.VMEM((2, 2 * half, 2 * LANES), jnp.float32),
+    ]
     return vmem_call(mixer_kernel, outs, scratch)(
         *rows, packed, taps, paired_blocks(gate_a_weight), paired_blocks(gate_x_weight), rate
     )
@@ -527,8 +540,8 @@
     downs = full_tiles(0, 5) + [((0, 640, HALF),)]
     order = gates + uppers + ends
     mixing = full_tiles(3, 1) + full_tiles(4, 1) + [((3, LANES, HALF), (4, LANES, HALF))]
-    mixing += full_tiles(5, 1) + [((5, LANES, HALF),)]
-    from_two = [tuple((which + 6, at, size) for which, at, size in p) for p in downs + order]
+    mixing += full_tiles(5, 1) + [((5, LANES, HALF), (6, 640, HALF))]
+    from_two = [tuple((which + 6, at, size) for which, at, size in p) for p in downs[:5] + order]
     own, others, mixing, second = packed_tiles(
         downs + order + mixing + from_two,
         [
@@ -536,7 +549,7 @@
             *(lru_in_weight, lru_gate_weight, mix_out_weight.T),
             *(ffn2_down.T, ffn2_gate, ffn2_up),
         ],
-        (8, 9, 5, 17),
+        (8, 9, 5, 16),
         (1, 1, 1, 1),
     )
     packed_mixing = gather_tiles(mixing)
@@ -552,12 +565,13 @@
     first, normed = combined(tokens, sums, True, "zy", mix_gain)
     packed_mixing = fetched(packed_mixing)
     rows = gather_rows(normed)
-    sums = sent_sums(
-        mixer_terms(rows, packed_mixing, conv_weight, gate_a_weight, gate_x_weight, decay_param),
+    terms = mixer_terms(
+        rows, packed_mixing, conv_weight, gate_a_weight, gate_x_weight, decay_param
     )
+    sums = last_sums(terms)
     second, normed = combined(first, sums, False, "", ffn2_gain)
     rows = gather_rows(normed)
-    sums = last_sums(ffn_terms(rows, packed))
+    sums = last_sums(ffn_terms(rows, packed_mixing, packed))
     return combined(second, sums, True)[0]
 
 

time: 229 us -> 231 us (level)
  blocking collectives: 60.8 us -> 47.7 us
  waiting for transfers between devices: 76.3 us -> 85 us
  starting transfers between devices: 55 us -> 58.4 us
    all_to_all x1 -> x0, blocking collectives: 14.4 us -> none  [sent_sums(): return [lax.all_to_all(sums, 'x', split_axis=0, concat_axis=0, tiled=True)]]
    ppermute x27 -> x30, waiting for transfers between devices: 63.7 us -> 72.3 us  [moved(): lax.ppermute(value, axis, [(i, (i - by) % count) for i in range(count)])]
    ppermute x27 -> x30, starting transfers between devices: 51.5 us -> 54.9 us  [moved(): lax.ppermute(value, axis, [(i, (i - by) % count) for i in range(count)])]
  transfers between devices with their start and end apart: 30 -> 33, of which waited for: 16 -> 18; matrix products, arithmetic and copies ran while one was open for 0% -> 0% of each run, Pallas kernels for 6% -> 6%
where the time goes in v3:
time: 231 us
  waiting for transfers between devices  85 us (37%)
  starting transfers between devices  58.4 us (25%)
  blocking collectives  47.7 us (21%)
  Pallas kernels  24 us (10%)
  between operations  13.7 us (6%)
    ppermute x30, waiting for transfers between devices, moved(): lax.ppermute(value, axis, [(i, (i - by) % count) for i in range(count)])  72.3 us
    ppermute x30, starting transfers between devices, moved(): lax.ppermute(value, axis, [(i, (i - by) % count) for i in range(count)])  54.9 us
    all_gather x3, blocking collectives, gather_rows(): mine = lax.all_gather(own, 'x', axis=0, tiled=True)  36.3 us
    pallas_call x10, Pallas kernels, call(): pl.pallas_call(kernel, in_specs=vmem_specs(len(args)), out_specs=jax.tree...  13.5 us
    all_to_all x1, waiting for transfers between devices, sent_sums(): return [lax.all_to_all(sums, 'x', split_axis=0, concat_axis=0, tiled=True)]  11.9 us
    all_gather x1, blocking collectives, body(): own = lax.all_gather(own, 'y', axis=0)  11.4 us
    pallas_call x1, Pallas kernels, ffn_terms(): pl.pallas_call(ffn_kernel, in_specs=vmem_specs(3) + [pl.BlockSpec(memory_...  6.6 us
  transfers between devices with their start and end apart: 33, of which 18 were waited for; matrix products, arithmetic and copies ran while one was open for 0% of the time, Pallas kernels for 6%

profile of v3, /device:TPU:1, one launch (start us, length us, event | category | flops | bytes accessed | tf_op | source)
XLA Modules:
  0.0 231.2 jit_solution(2796902152305634644)
XLA Ops:
  9.4 6.5 %collective-permute-start = (bf16[9,64,128]{2,1,0:T(8,128)(2,1)S(1)}, bf16[9,64,128]{2,1,0:T(8,128)(2,1)S(1)}, u32[]{:S(2)}, u32[]{:S(2)}) collective-permute-start(bf16[9,64,128]{2,1,0:T(8,128)(2,1)S(1)} %get-tuple-element.43.refs_0_), channel_id=1, source_target_pairs={{0,224},{32,0},{64,32},{96,64},{128,96},{160,128},{192,160},{224,1... | collective-permute-start | bytes 442376 | tf_op jit(solution)/shard_map/ppermute | solution.py:23
  18.4 3.1 %collective-permute-done.1.refs_7_ = bf16[9,64,128]{2,1,0:T(8,128)(2,1)S(1)} collective-permute-done((bf16[9,64,128]{2,1,0:T(8,128)(2,1)S(1)}, bf16[9,64,128]{2,1,0:T(8,128)(2,1)S(1)}, u32[]{:S(2)}, u32[]{:S(2)}) %collective-permute-start.1) | collective-permute-done | bytes 147488 | tf_op jit(solution)/shard_map/ppermute | solution.py:23
  28.5 11.4 %all-gather = bf16[32,64,128]{2,1,0:T(8,128)(2,1)S(1)} all-gather(bf16[8,64,128]{2,1,0:T(8,128)(2,1)S(1)} %get-tuple-element.51), channel_id=2, replica_groups=mesh['z'=8,'y'=4,'x'=4,'c'=2] {'y'}, dimensions={0}, use_global_device_ids=true | all-gather | bytes 655360 | tf_op jit(solution)/shard_map/all_gather | solution.py:557
  41.5 2.6 %collective-permute-start.6 = (bf16[9,64,128]{2,1,0:T(8,128)(2,1)S(1)}, bf16[9,64,128]{2,1,0:T(8,128)(2,1)S(1)}, u32[]{:S(2)}, u32[]{:S(2)}) collective-permute-start(bf16[9,64,128]{2,1,0:T(8,128)(2,1)S(1)} %collective-permute-done.4.refs_3_), channel_id=1, source_target_pairs={{0,224},{32,0},{64,32},{96,64},{128,96},{160,128},{192,160},{224,1... | collective-permute-start | bytes 442376 | tf_op jit(solution)/shard_map/ppermute | solution.py:23
  44.1 8.9 %collective-permute-done.6.refs_4_ = bf16[9,64,128]{2,1,0:T(8,128)(2,1)S(1)} collective-permute-done((bf16[9,64,128]{2,1,0:T(8,128)(2,1)S(1)}, bf16[9,64,128]{2,1,0:T(8,128)(2,1)S(1)}, u32[]{:S(2)}, u32[]{:S(2)}) %collective-permute-start.6) | collective-permute-done | bytes 147488 | tf_op jit(solution)/shard_map/ppermute | solution.py:23
  53.1 3.2 %collective-permute-start.15 = (bf16[8,9,64,128]{3,2,1,0:T(8,128)(2,1)S(1)}, bf16[8,9,64,128]{3,2,1,0:T(8,128)(2,1)S(1)}, u32[]{:S(2)}, u32[]{:S(2)}) collective-permute-start(bf16[8,9,64,128]{3,2,1,0:T(8,128)(2,1)S(1)} %shard_map.164.refs_8_), channel_id=1, source_target_pairs={{0,24},{8,0},{16,8},{24,16},{1,25},{9,1},{17,9},{25,17},{2,26},{10... | collective-permute-start | bytes 3538952 | tf_op jit(solution)/shard_map/ppermute | solution.py:23
  56.3 3.2 %collective-permute-start.10 = (bf16[4,8,64,128]{3,2,1,0:T(8,128)(2,1)S(1)}, bf16[4,8,64,128]{3,2,1,0:T(8,128)(2,1)S(1)}, u32[]{:S(2)}, u32[]{:S(2)}) collective-permute-start(bf16[4,8,64,128]{3,2,1,0:T(8,128)(2,1)S(1)} %collective-permute-done.8.refs_1_), channel_id=1, source_target_pairs={{0,224},{32,0},{64,32},{96,64},{128,96},{160,128},{192,160},{224,1... | collective-permute-start | bytes 1572872 | tf_op jit(solution)/shard_map/ppermute | solution.py:23
  59.9 9.4 %collective-permute-done.10.refs_2_ = bf16[4,8,64,128]{3,2,1,0:T(8,128)(2,1)S(1)} collective-permute-done((bf16[4,8,64,128]{3,2,1,0:T(8,128)(2,1)S(1)}, bf16[4,8,64,128]{3,2,1,0:T(8,128)(2,1)S(1)}, u32[]{:S(2)}, u32[]{:S(2)}) %collective-permute-start.10) | collective-permute-done | bytes 524320 | tf_op jit(solution)/shard_map/ppermute | solution.py:23
  69.3 3.3 %collective-permute-done.11.refs_6_ = bf16[4,8,64,128]{3,2,1,0:T(8,128)(2,1)S(1)} collective-permute-done((bf16[4,8,64,128]{3,2,1,0:T(8,128)(2,1)S(1)}, bf16[4,8,64,128]{3,2,1,0:T(8,128)(2,1)S(1)}, u32[]{:S(2)}, u32[]{:S(2)}) %collective-permute-start.11) | collective-permute-done | bytes 524320 | tf_op jit(solution)/shard_map/ppermute | solution.py:23
  74.1 12.1 %all_gather.21.mine_ref = bf16[192,2048]{1,0:T(8,128)(2,1)S(1)} all-gather(bf16[48,2048]{1,0:T(8,128)(2,1)S(1)} %shard_map.163), channel_id=1, replica_groups=mesh['z'=8,'y'=4,'x'=4,'c'=2] {'x'}, dimensions={0}, use_global_device_ids=true | all-gather | bytes 983040 | tf_op jit(solution)/shard_map/all_gather | solution.py:93
  86.2 10.1 %collective-permute-start.7 = (bf16[192,2048]{1,0:T(8,128)(2,1)S(1)}, bf16[192,2048]{1,0:T(8,128)(2,1)S(1)}, u32[]{:S(2)}, u32[]{:S(2)}) collective-permute-start(bf16[192,2048]{1,0:T(8,128)(2,1)S(1)} %all_gather.21.mine_ref), channel_id=1, source_target_pairs={{0,1},{1,0},{2,3},{3,2},{4,5},{5,4},{6,7},{7,6},{8,9},{9,8},{10,11... | collective-permute-start | bytes 2359304 | tf_op jit(solution)/shard_map/ppermute | solution.py:23
  96.3 5.9 %collective-permute-start.17 = (bf16[8,5,64,128]{3,2,1,0:T(8,128)(2,1)S(1)}, bf16[8,5,64,128]{3,2,1,0:T(8,128)(2,1)S(1)}, u32[]{:S(2)}, u32[]{:S(2)}) collective-permute-start(bf16[8,5,64,128]{3,2,1,0:T(8,128)(2,1)S(1)} %slice.24), channel_id=1, source_target_pairs={{0,24},{8,0},{16,8},{24,16},{1,25},{9,1},{17,9},{25,17},{2,26},{10... | collective-permute-start | bytes 1966088 | tf_op jit(solution)/shard_map/ppermute | solution.py:23
  103.4 15.3 %collective-permute-done.18.refs_11_ = bf16[8,4,64,128]{3,2,1,0:T(8,128)(2,1)S(1)} collective-permute-done((bf16[8,4,64,128]{3,2,1,0:T(8,128)(2,1)S(1)}, bf16[8,4,64,128]{3,2,1,0:T(8,128)(2,1)S(1)}, u32[]{:S(2)}, u32[]{:S(2)}) %collective-permute-start.18) | collective-permute-done | bytes 524320 | tf_op jit(solution)/shard_map/ppermute | solution.py:23
  119.1 3.8 %shard_map.165 = (bf16[192,2048]{1,0:T(8,128)(2,1)S(1)}, bf16[192,2048]{1,0:T(8,128)(2,1)S(1)}) custom-call(bf16[192,2048]{1,0:T(8,128)(2,1)S(1)} %all_gather.21.mine_ref, bf16[192,2048]{1,0:T(8,128)(2,1)S(1)} %collective-permute-done.7.other_ref, bf16[4,8,64,128]{3,2,1,0:T(8,128)(2,1)S(1)} %bitcast.34, ...), custom_call_target="tpu_custom_call" | custom-call | tf_op jit(solution)/shard_map/pallas_call | solution.py:36
  127.7 3.5 %all-to-all-start = ((bf16[4,48,2048]{2,1,0:T(8,128)(2,1)}), bf16[4,48,2048]{2,1,0:T(8,128)(2,1)S(1)}, u32[]{:S(2)}, u32[]{:S(2)}) async-start(bf16[4,48,2048]{2,1,0:T(8,128)(2,1)} %shard_map.166), calls=%async_computation | async-start | bytes 1572864 | tf_op jit(solution)/shard_map/all_to_all | solution.py:112
  131.2 11.9 %all-to-all-done.refs_1_ = bf16[4,48,2048]{2,1,0:T(8,128)(2,1)S(1)} async-done(((bf16[4,48,2048]{2,1,0:T(8,128)(2,1)}), bf16[4,48,2048]{2,1,0:T(8,128)(2,1)S(1)}, u32[]{:S(2)}, u32[]{:S(2)}) %all-to-all-start) | async-done | bytes 786464 | tf_op jit(solution)/shard_map/all_to_all | solution.py:112
  143.7 11.4 %all_gather.24.mine_ref = bf16[192,2048]{1,0:T(8,128)(2,1)S(1)} all-gather(bf16[48,2048]{1,0:T(8,128)(2,1)S(1)} %get-tuple-element.64), channel_id=1, replica_groups=mesh['z'=8,'y'=4,'x'=4,'c'=2] {'x'}, dimensions={0}, use_global_device_ids=true | all-gather | bytes 983040 | tf_op jit(solution)/shard_map/all_gather | solution.py:93
  155.1 4.0 %collective-permute-start.20 = (bf16[192,2048]{1,0:T(8,128)(2,1)S(1)}, bf16[192,2048]{1,0:T(8,128)(2,1)}, u32[]{:S(2)}, u32[]{:S(2)}) collective-permute-start(bf16[192,2048]{1,0:T(8,128)(2,1)S(1)} %all_gather.24.mine_ref), channel_id=1, source_target_pairs={{0,1},{1,0},{2,3},{3,2},{4,5},{5,4},{6,7},{7,6},{8,9},{9,8},{10,11... | collective-permute-start | bytes 2359304 | tf_op jit(solution)/shard_map/ppermute | solution.py:23
  161.2 6.2 %shard_map.168 = (bf16[192,2048]{1,0:T(8,128)(2,1)S(1)}, bf16[192,2048]{1,0:T(8,128)(2,1)S(1)}) custom-call(bf16[192,2048]{1,0:T(8,128)(2,1)S(1)} %all_gather.24.mine_ref, bf16[192,2048]{1,0:T(8,128)(2,1)} %collective-permute-done.20.other_ref, bf16[32,5,64,128]{3,2,1,0:T(8,128)(2,1)S(1)} %copy_in.1.packed_ref.mixing_ref, ...), custom_call_target="tpu_custom_call" | custom-call | tf_op jit(solution)/shard_map/pallas_call | solution.py:36
  173.3 8.5 %collective-permute-done.22.refs_2_ = bf16[48,2048]{1,0:T(8,128)(2,1)S(1)} collective-permute-done((bf16[48,2048]{1,0:T(8,128)(2,1)S(1)}, bf16[48,2048]{1,0:T(8,128)(2,1)S(1)}, u32[]{:S(2)}, u32[]{:S(2)}) %collective-permute-start.22) | collective-permute-done | bytes 196640 | tf_op jit(solution)/shard_map/ppermute | solution.py:23
  182.4 12.8 %all_gather.26.mine_ref = bf16[192,2048]{1,0:T(8,128)(2,1)S(1)} all-gather(bf16[48,2048]{1,0:T(8,128)(2,1)S(1)} %get-tuple-element.73), channel_id=1, replica_groups=mesh['z'=8,'y'=4,'x'=4,'c'=2] {'x'}, dimensions={0}, use_global_device_ids=true | all-gather | bytes 983040 | tf_op jit(solution)/shard_map/all_gather | solution.py:93
  201.0 6.6 %ffn.1 = (bf16[192,2048]{1,0:T(8,128)(2,1)S(1)}, bf16[192,2048]{1,0:T(8,128)(2,1)S(1)}) custom-call(bf16[192,2048]{1,0:T(8,128)(2,1)S(1)} %all_gather.26.mine_ref, bf16[192,2048]{1,0:T(8,128)(2,1)S(1)} %copy-done.1, bf16[32,5,64,128]{3,2,1,0:T(8,128)(2,1)S(1)} %copy_in.1.packed_ref.mixing_ref, bf16[32,16,64,128]{3,2,1,0:T(8,128)(2,1)} %bitcast.38), custom_call_target="tpu_custom_call" | custom-call | tf_op jit(solution)/shard_map/ffn/pallas_call | solution.py:396
  214.7 3.6 %collective-permute-done.27.refs_2_ = bf16[48,2048]{1,0:T(8,128)(2,1)S(1)} collective-permute-done((bf16[48,2048]{1,0:T(8,128)(2,1)S(1)}, bf16[48,2048]{1,0:T(8,128)(2,1)S(1)}, u32[]{:S(2)}, u32[]{:S(2)}) %collective-permute-start.27) | collective-permute-done | bytes 196640 | tf_op jit(solution)/shard_map/ppermute | solution.py:23
  218.4 5.1 %collective-permute-done.28.refs_3_ = bf16[48,2048]{1,0:T(8,128)(2,1)S(1)} collective-permute-done((bf16[48,2048]{1,0:T(8,128)(2,1)S(1)}, bf16[48,2048]{1,0:T(8,128)(2,1)S(1)}, u32[]{:S(2)}, u32[]{:S(2)}) %collective-permute-start.28) | collective-permute-done | bytes 196640 | tf_op jit(solution)/shard_map/ppermute | solution.py:23
  (100 shorter events, 44.9 us)
Async XLA Ops:
  6.5 152.8 %all-gather.4.cloned.1.call-start = ((), (), s32[]{:S(2)}) async-start(), calls=%async_computation.1 | async-start | bytes 2703360 | tf_op jit(solution)/shard_map/all_gather | solution.py:195
  8.7 191.2 %all-gather.6.cloned.1.call-start = ((), (), s32[]{:S(2)}) async-start(), calls=%async_computation.2 | async-start | bytes 8650752 | tf_op jit(solution)/shard_map/all_gather | solution.py:195
  9.4 9.0 %collective-permute-start = (bf16[9,64,128]{2,1,0:T(8,128)(2,1)S(1)}, bf16[9,64,128]{2,1,0:T(8,128)(2,1)S(1)}, u32[]{:S(2)}, u32[]{:S(2)}) collective-permute-start(bf16[9,64,128]{2,1,0:T(8,128)(2,1)S(1)} %get-tuple-element.43.refs_0_), channel_id=1, source_target_pairs={{0,224},{32,0},{64,32},{96,64},{128,96},{160,128},{192,160},{224,1... | collective-permute-start | bytes 442376 | tf_op jit(solution)/shard_map/ppermute | solution.py:23
  27.0 12.9 %collective-permute-start.4 = (bf16[9,64,128]{2,1,0:T(8,128)(2,1)S(1)}, bf16[9,64,128]{2,1,0:T(8,128)(2,1)S(1)}, u32[]{:S(2)}, u32[]{:S(2)}) collective-permute-start(bf16[9,64,128]{2,1,0:T(8,128)(2,1)S(1)} %collective-permute-done.2.refs_2_), channel_id=1, source_target_pairs={{0,224},{32,0},{64,32},{96,64},{128,96},{160,128},{192,160},{224,1... | collective-permute-start | bytes 442376 | tf_op jit(solution)/shard_map/ppermute | solution.py:23
  27.0 12.9 %collective-permute-start.5 = (bf16[9,64,128]{2,1,0:T(8,128)(2,1)S(1)}, bf16[9,64,128]{2,1,0:T(8,128)(2,1)S(1)}, u32[]{:S(2)}, u32[]{:S(2)}) collective-permute-start(bf16[9,64,128]{2,1,0:T(8,128)(2,1)S(1)} %collective-permute-done.3.refs_6_), channel_id=1, source_target_pairs={{0,32},{32,64},{64,96},{96,128},{128,160},{160,192},{192,224},{224... | collective-permute-start | bytes 442376 | tf_op jit(solution)/shard_map/ppermute | solution.py:23
  39.9 16.3 %collective-permute-start.8 = (bf16[4,8,64,128]{3,2,1,0:T(8,128)(2,1)S(1)}, bf16[4,8,64,128]{3,2,1,0:T(8,128)(2,1)S(1)}, u32[]{:S(2)}, u32[]{:S(2)}) collective-permute-start(bf16[4,8,64,128]{3,2,1,0:T(8,128)(2,1)S(1)} %bitcast.32), channel_id=1, source_target_pairs={{0,224},{32,0},{64,32},{96,64},{128,96},{160,128},{192,160},{224,1... | collective-permute-start | bytes 1572872 | tf_op jit(solution)/shard_map/ppermute | solution.py:23
  41.4 14.9 %collective-permute-start.9 = (bf16[4,8,64,128]{3,2,1,0:T(8,128)(2,1)S(1)}, bf16[4,8,64,128]{3,2,1,0:T(8,128)(2,1)S(1)}, u32[]{:S(2)}, u32[]{:S(2)}) collective-permute-start(bf16[4,8,64,128]{3,2,1,0:T(8,128)(2,1)S(1)} %bitcast.33), channel_id=1, source_target_pairs={{0,32},{32,64},{64,96},{96,128},{128,160},{160,192},{192,224},{224... | collective-permute-start | bytes 1572872 | tf_op jit(solution)/shard_map/ppermute | solution.py:23
  41.5 11.5 %collective-permute-start.6 = (bf16[9,64,128]{2,1,0:T(8,128)(2,1)S(1)}, bf16[9,64,128]{2,1,0:T(8,128)(2,1)S(1)}, u32[]{:S(2)}, u32[]{:S(2)}) collective-permute-start(bf16[9,64,128]{2,1,0:T(8,128)(2,1)S(1)} %collective-permute-done.4.refs_3_), channel_id=1, source_target_pairs={{0,224},{32,0},{64,32},{96,64},{128,96},{160,128},{192,160},{224,1... | collective-permute-start | bytes 442376 | tf_op jit(solution)/shard_map/ppermute | solution.py:23
  53.1 43.2 %collective-permute-start.15 = (bf16[8,9,64,128]{3,2,1,0:T(8,128)(2,1)S(1)}, bf16[8,9,64,128]{3,2,1,0:T(8,128)(2,1)S(1)}, u32[]{:S(2)}, u32[]{:S(2)}) collective-permute-start(bf16[8,9,64,128]{3,2,1,0:T(8,128)(2,1)S(1)} %shard_map.164.refs_8_), channel_id=1, source_target_pairs={{0,24},{8,0},{16,8},{24,16},{1,25},{9,1},{17,9},{25,17},{2,26},{10... | collective-permute-start | bytes 3538952 | tf_op jit(solution)/shard_map/ppermute | solution.py:23
  56.3 40.0 %collective-permute-start.16 = (bf16[8,9,64,128]{3,2,1,0:T(8,128)(2,1)S(1)}, bf16[8,9,64,128]{3,2,1,0:T(8,128)(2,1)S(1)}, u32[]{:S(2)}, u32[]{:S(2)}) collective-permute-start(bf16[8,9,64,128]{3,2,1,0:T(8,128)(2,1)S(1)} %shard_map.164.refs_8_), channel_id=1, source_target_pairs={{0,8},{8,16},{16,24},{24,0},{1,9},{9,17},{17,25},{25,1},{2,10},{10... | collective-permute-start | bytes 3538952 | tf_op jit(solution)/shard_map/ppermute | solution.py:23
  56.3 13.0 %collective-permute-start.10 = (bf16[4,8,64,128]{3,2,1,0:T(8,128)(2,1)S(1)}, bf16[4,8,64,128]{3,2,1,0:T(8,128)(2,1)S(1)}, u32[]{:S(2)}, u32[]{:S(2)}) collective-permute-start(bf16[4,8,64,128]{3,2,1,0:T(8,128)(2,1)S(1)} %collective-permute-done.8.refs_1_), channel_id=1, source_target_pairs={{0,224},{32,0},{64,32},{96,64},{128,96},{160,128},{192,160},{224,1... | collective-permute-start | bytes 1572872 | tf_op jit(solution)/shard_map/ppermute | solution.py:23
  59.5 13.1 %collective-permute-start.11 = (bf16[4,8,64,128]{3,2,1,0:T(8,128)(2,1)S(1)}, bf16[4,8,64,128]{3,2,1,0:T(8,128)(2,1)S(1)}, u32[]{:S(2)}, u32[]{:S(2)}) collective-permute-start(bf16[4,8,64,128]{3,2,1,0:T(8,128)(2,1)S(1)} %collective-permute-done.9.refs_7_), channel_id=1, source_target_pairs={{0,32},{32,64},{64,96},{96,128},{128,160},{160,192},{192,224},{224... | collective-permute-start | bytes 1572872 | tf_op jit(solution)/shard_map/ppermute | solution.py:23
  72.6 29.8 %collective-permute-start.12 = (bf16[4,8,64,128]{3,2,1,0:T(8,128)(2,1)S(1)}, bf16[4,8,64,128]{3,2,1,0:T(8,128)(2,1)S(1)}, u32[]{:S(2)}, u32[]{:S(2)}) collective-permute-start(bf16[4,8,64,128]{3,2,1,0:T(8,128)(2,1)S(1)} %collective-permute-done.10.refs_2_), channel_id=1, source_target_pairs={{0,224},{32,0},{64,32},{96,64},{128,96},{160,128},{192,160},{224,1... | collective-permute-start | bytes 1572872 | tf_op jit(solution)/shard_map/ppermute | solution.py:23
  72.8 29.6 %collective-permute-start.13 = (bf16[4,8,64,128]{3,2,1,0:T(8,128)(2,1)S(1)}, bf16[4,8,64,128]{3,2,1,0:T(8,128)(2,1)S(1)}, u32[]{:S(2)}, u32[]{:S(2)}) collective-permute-start(bf16[4,8,64,128]{3,2,1,0:T(8,128)(2,1)S(1)} %collective-permute-done.11.refs_6_), channel_id=1, source_target_pairs={{0,32},{32,64},{64,96},{96,128},{128,160},{160,192},{192,224},{224... | collective-permute-start | bytes 1572872 | tf_op jit(solution)/shard_map/ppermute | solution.py:23
  86.2 17.2 %collective-permute-start.7 = (bf16[192,2048]{1,0:T(8,128)(2,1)S(1)}, bf16[192,2048]{1,0:T(8,128)(2,1)S(1)}, u32[]{:S(2)}, u32[]{:S(2)}) collective-permute-start(bf16[192,2048]{1,0:T(8,128)(2,1)S(1)} %all_gather.21.mine_ref), channel_id=1, source_target_pairs={{0,1},{1,0},{2,3},{3,2},{4,5},{5,4},{6,7},{7,6},{8,9},{9,8},{10,11... | collective-permute-start | bytes 2359304 | tf_op jit(solution)/shard_map/ppermute | solution.py:23
  96.3 22.8 %collective-permute-start.17 = (bf16[8,5,64,128]{3,2,1,0:T(8,128)(2,1)S(1)}, bf16[8,5,64,128]{3,2,1,0:T(8,128)(2,1)S(1)}, u32[]{:S(2)}, u32[]{:S(2)}) collective-permute-start(bf16[8,5,64,128]{3,2,1,0:T(8,128)(2,1)S(1)} %slice.24), channel_id=1, source_target_pairs={{0,24},{8,0},{16,8},{24,16},{1,25},{9,1},{17,9},{25,17},{2,26},{10... | collective-permute-start | bytes 1966088 | tf_op jit(solution)/shard_map/ppermute | solution.py:23
  102.3 16.4 %collective-permute-start.18 = (bf16[8,4,64,128]{3,2,1,0:T(8,128)(2,1)S(1)}, bf16[8,4,64,128]{3,2,1,0:T(8,128)(2,1)S(1)}, u32[]{:S(2)}, u32[]{:S(2)}) collective-permute-start(bf16[8,4,64,128]{3,2,1,0:T(8,128)(2,1)S(1)} %slice.25), channel_id=1, source_target_pairs={{0,8},{8,16},{16,24},{24,0},{1,9},{9,17},{17,25},{25,1},{2,10},{10... | collective-permute-start | bytes 1572872 | tf_op jit(solution)/shard_map/ppermute | solution.py:23
  102.4 16.7 %collective-permute-start.14 = (bf16[4,8,64,128]{3,2,1,0:T(8,128)(2,1)S(1)}, bf16[4,8,64,128]{3,2,1,0:T(8,128)(2,1)S(1)}, u32[]{:S(2)}, u32[]{:S(2)}) collective-permute-start(bf16[4,8,64,128]{3,2,1,0:T(8,128)(2,1)S(1)} %collective-permute-done.12.refs_3_), channel_id=1, source_target_pairs={{0,224},{32,0},{64,32},{96,64},{128,96},{160,128},{192,160},{224,1... | collective-permute-start | bytes 1572872 | tf_op jit(solution)/shard_map/ppermute | solution.py:23
  127.7 15.5 %all-to-all-start = ((bf16[4,48,2048]{2,1,0:T(8,128)(2,1)}), bf16[4,48,2048]{2,1,0:T(8,128)(2,1)S(1)}, u32[]{:S(2)}, u32[]{:S(2)}) async-start(bf16[4,48,2048]{2,1,0:T(8,128)(2,1)} %shard_map.166), calls=%async_computation | async-start | bytes 1572864 | tf_op jit(solution)/shard_map/all_to_all | solution.py:112
  170.0 11.8 %collective-permute-start.22 = (bf16[48,2048]{1,0:T(8,128)(2,1)S(1)}, bf16[48,2048]{1,0:T(8,128)(2,1)S(1)}, u32[]{:S(2)}, u32[]{:S(2)}) collective-permute-start(bf16[48,2048]{1,0:T(8,128)(2,1)S(1)} %get-tuple-element.69), channel_id=1, source_target_pairs={{0,2},{2,4},{4,6},{6,0},{1,3},{3,5},{5,7},{7,1},{8,10},{10,12},{12... | collective-permute-start | bytes 589832 | tf_op jit(solution)/shard_map/ppermute | solution.py:23
  170.0 11.7 %collective-permute-start.23 = (bf16[48,2048]{1,0:T(8,128)(2,1)S(1)}, bf16[48,2048]{1,0:T(8,128)(2,1)S(1)}, u32[]{:S(2)}, u32[]{:S(2)}) collective-permute-start(bf16[48,2048]{1,0:T(8,128)(2,1)S(1)} %get-tuple-element.70), channel_id=1, source_target_pairs={{0,4},{2,6},{4,0},{6,2},{1,5},{3,7},{5,1},{7,3},{8,12},{10,14},{12... | collective-permute-start | bytes 589832 | tf_op jit(solution)/shard_map/ppermute | solution.py:23
  171.8 10.3 %collective-permute-start.24 = (bf16[48,2048]{1,0:T(8,128)(2,1)S(1)}, bf16[48,2048]{1,0:T(8,128)(2,1)S(1)}, u32[]{:S(2)}, u32[]{:S(2)}) collective-permute-start(bf16[48,2048]{1,0:T(8,128)(2,1)S(1)} %get-tuple-element.71), channel_id=1, source_target_pairs={{0,6},{2,0},{4,2},{6,4},{1,7},{3,1},{5,3},{7,5},{8,14},{10,8},{12,... | collective-permute-start | bytes 589832 | tf_op jit(solution)/shard_map/ppermute | solution.py:23
  212.3 11.2 %collective-permute-start.28 = (bf16[48,2048]{1,0:T(8,128)(2,1)S(1)}, bf16[48,2048]{1,0:T(8,128)(2,1)S(1)}, u32[]{:S(2)}, u32[]{:S(2)}) collective-permute-start(bf16[48,2048]{1,0:T(8,128)(2,1)S(1)} %get-tuple-element.79), channel_id=1, source_target_pairs={{0,4},{2,6},{4,0},{6,2},{1,5},{3,7},{5,1},{7,3},{8,12},{10,14},{12... | collective-permute-start | bytes 589832 | tf_op jit(solution)/shard_map/ppermute | solution.py:23
  214.6 8.8 %collective-permute-start.29 = (bf16[48,2048]{1,0:T(8,128)(2,1)S(1)}, bf16[48,2048]{1,0:T(8,128)(2,1)S(1)}, u32[]{:S(2)}, u32[]{:S(2)}) collective-permute-start(bf16[48,2048]{1,0:T(8,128)(2,1)S(1)} %get-tuple-element.80), channel_id=1, source_target_pairs={{0,6},{2,0},{4,2},{6,4},{1,7},{3,1},{5,3},{7,5},{8,14},{10,8},{12,... | collective-permute-start | bytes 589832 | tf_op jit(solution)/shard_map/ppermute | solution.py:23
  (23 other events, 343.8 us)
Sparse Core Ops, SparseCore 0:
  9.9 85.2 all-gather.3
  97.8 95.7 all-gather.5
